TPU v7x, 256 devices: a whole 4x4x8 slice. The times are simulated.
256 devices in a mesh: kv: 32 (over z, x), tp: 8 (over y, core).
Axes of the slice: x: 4, y: 4, z: 8, core: 2. Of those that a mesh axis runs over, the one named last changes fastest.
Arguments:
- tokens: bfloat16 [256, 2048], P(None, 'kv'), may hold values from -16 to 16
- norm_gain: float32 [2048], P('kv'), may hold values from 0.1 to 1.9
- query_weight: bfloat16 [2048, 2048], P('kv', 'tp'), may hold values from -0.125 to 0.125
- key_weight: bfloat16 [2048, 2048], P('kv', 'tp'), may hold values from -0.125 to 0.125
- value_weight: bfloat16 [2048, 2048], P('kv', 'tp'), may hold values from -0.125 to 0.125
- gate_weight: bfloat16 [2048, 2048], P('kv', 'tp'), may hold values from -0.125 to 0.125
- beta_weight: bfloat16 [2048, 16], replicated, may hold values from -0.125 to 0.125
- decay_weight: bfloat16 [2048, 16], replicated, may hold values from -0.5 to 0.5
- decay_rate: float32 [16], P('tp'), may hold values from 0.0005 to 0.1
- head_gain: float32 [128], replicated, may hold values from 0.1 to 1.9
- carried_state: float32 [256, 16, 128, 128], P('kv', 'tp'), may hold values from -4 to 4
- block_keys: bfloat16 [256, 16, 64, 128], P('kv', 'tp'), may hold values from -1 to 1, as said below
- block_values: bfloat16 [256, 16, 64, 128], P('kv', 'tp'), may hold values from -6 to 6
- block_beta: float32 [256, 16, 64], P('kv', 'tp'), may hold values from 0.1 to 0.9
- block_decay: float32 [256, 16, 64], P('kv', 'tp'), may hold values from -1.2 to 0
- live_count: int32 [256], P('kv'), may hold values from 1 to 64, 6553 in all
- out_weight: bfloat16 [2048, 2048], P('tp', 'kv'), may hold values from -0.125 to 0.125
- mlp_gain: float32 [2048], replicated, may hold values from 0.1 to 1.9
- up_weight: bfloat16 [2048, 8192], P('kv', 'tp'), may hold values from -0.125 to 0.125
- down_weight: bfloat16 [8192, 2048], P('tp', 'kv'), may hold values from -0.0625 to 0.0625
Outputs:
- mixed: bfloat16 [256, 2048], P(None, 'kv')
- new_state: float32 [256, 16, 128, 128], P('kv', 'tp')
Inputs may be any that keep to these rules, and one draw needn't show every extreme that they name: `block_keys`: every key vector along the last dimension has unit length up to rounding.
All inputs are finite; a program needn't handle non-finite values. No bound on the sum of `live_count` on one device may be relied on, other than what follows from the above.
Results may differ from a plain program's by a relative error of at most 0.023.
Values may be sent and summed in bfloat16 or wider, within the bound.
A program may use at most 64 MiB of HBM per device.

v0:
```python
import jax
import jax.numpy as jnp
from jax import lax
from jax.sharding import PartitionSpec as P

MODEL = 2048


EPS = 1e-06
PRECISE = lax.Precision.HIGHEST


def in_blocks(x, dim, devices):
    dims = x.shape
    tiles = x.reshape(*dims[:dim], devices, dims[dim] // devices, *dims[dim + 1 :])
    return jnp.moveaxis(tiles, dim, 0)


def sent_and_summed(x, axis, dim):
    devices = lax.axis_size(axis)
    tiles = lax.all_to_all(in_blocks(x, dim, devices), axis, 0, 0, tiled=True)
    return jnp.sum(tiles.astype(jnp.float32), axis=0)


def side_by_side(arrays, axis, dim, along):
    columns = [a.reshape(*a.shape[:along], -1) for a in arrays]
    both = jnp.concatenate(columns, axis=along)
    whole, at, gathered = (sent_and_summed(both, axis, dim), 0, [])
    for a, column in zip(arrays, columns):
        piece = whole[..., at : at + column.shape[along]]
        gathered.append(piece.reshape(*piece.shape[:along], *a.shape[along:]))
        at += column.shape[along]
    return tuple(gathered)


def in_order(tiles, dim):
    dims = list(tiles.shape[1:])
    dims[dim] *= tiles.shape[0]
    return jnp.moveaxis(tiles, 0, dim).reshape(dims)


def sent_to_all(x, axis):
    copies = jnp.broadcast_to(x, (lax.axis_size(axis), *x.shape))
    return lax.all_to_all(copies, axis, split_axis=0, concat_axis=0, tiled=True)


def collect(x, axis, dim):
    return in_order(sent_to_all(x, axis), dim)


def over_copies(x, axis):
    return sent_to_all(x, axis).astype(jnp.float32).sum(axis=0)


def unit_inverse(strict_lower):
    slots_count = strict_lower.shape[-1]
    identity = jnp.eye(slots_count, dtype=strict_lower.dtype)
    powered = -strict_lower
    product_sum = identity + powered
    for repeat in range(slots_count.bit_length() - 2):
        powered = jnp.matmul(powered, powered, precision=PRECISE)
        product_sum = product_sum + jnp.matmul(product_sum, powered, precision=PRECISE)
    return product_sum


def delta_block(
    queries,
    key_new,
    value_new,
    beta_new,
    decay_new,
    keys,
    values,
    betas,
    decays,
    live_count,
    carried_state,
):
    slots_count = keys.shape[2]
    slot_ids = jnp.arange(slots_count, dtype=jnp.int32)
    newest = (live_count - 1)[:, None, None]
    pending = slot_ids[None, None, :] < newest
    current = slot_ids[None, None, :] == newest
    keys_all = jnp.where(
        pending[..., None],
        keys,
        jnp.where(current[..., None], key_new[:, :, None, :], jnp.zeros_like(keys)),
    )
    values_all = jnp.where(
        pending[..., None],
        values,
        jnp.where(current[..., None], value_new[:, :, None, :], jnp.zeros_like(values)),
    )
    betas_all = jnp.where(pending, betas, jnp.where(current, beta_new[:, :, None], 0.0))
    decays_all = jnp.where(pending, decays, jnp.where(current, decay_new[:, :, None], 0.0))
    totals = jnp.cumsum(decays_all, axis=2)
    strict = slot_ids[:, None] > slot_ids[None, :]
    spread = jnp.where(strict, totals[..., :, None] - totals[..., None, :], 0.0)
    intersection = jnp.einsum(
        "shid,shjd->shij", keys_all, keys_all, preferred_element_type=jnp.float32
    )
    strict_lower = jnp.where(strict, betas_all[..., :, None] * intersection * jnp.exp(spread), 0.0)
    inverse = unit_inverse(strict_lower)
    key_vals = keys_all.astype(jnp.float32)
    right_values = betas_all[..., None] * values_all.astype(jnp.float32)
    right_keys = (betas_all * jnp.exp(totals))[..., None] * key_vals
    solved_values = jnp.einsum("shij,shjv->shiv", inverse, right_values, precision=PRECISE)
    solved_keys = jnp.einsum("shij,shjk->shik", inverse, right_keys, precision=PRECISE)
    update = solved_values - jnp.einsum(
        "shik,shkv->shiv", solved_keys, carried_state, precision=PRECISE
    )
    ending = totals[..., -1]
    faded_keys = key_vals * jnp.exp(ending[..., None] - totals)[..., None]
    new_state = jnp.exp(ending)[..., None, None] * carried_state + jnp.einsum(
        "shik,shiv->shkv", faded_keys, update, precision=PRECISE
    )
    readout = jnp.einsum("shk,shkv->shv", queries, new_state, precision=PRECISE)
    return (readout, new_state)


def body(
    tokens,
    norm_gain,
    query_weight,
    key_weight,
    value_weight,
    gate_weight,
    beta_weight,
    decay_weight,
    decay_rate,
    head_gain,
    carried_state,
    block_keys,
    block_values,
    block_beta,
    block_decay,
    live_count,
    out_weight,
    mlp_gain,
    up_weight,
    down_weight,
):
    kv_index = lax.axis_index("kv")
    tp_index = lax.axis_index("tp")
    columns = tokens.shape[1]
    seqs_here = carried_state.shape[0]
    heads_here = carried_state.shape[1]
    head_width = carried_state.shape[2]
    token_vals = tokens.astype(jnp.float32)
    squares = jnp.sum(token_vals * token_vals, axis=1)
    normed = (token_vals * norm_gain).astype(jnp.bfloat16)
    stacked = jnp.concatenate([query_weight, key_weight, value_weight, gate_weight], axis=1)
    beta_part = lax.dynamic_slice(
        beta_weight, (kv_index * columns, tp_index * heads_here), (columns, heads_here)
    )
    decay_part = lax.dynamic_slice(
        decay_weight, (kv_index * columns, tp_index * heads_here), (columns, heads_here)
    )
    small_weights = jnp.concatenate([beta_part, decay_part], axis=1)
    projected = jnp.dot(normed, stacked, preferred_element_type=jnp.float32)
    gating = jnp.dot(normed, small_weights, preferred_element_type=jnp.float32)
    projected, gating, squares = side_by_side(
        (projected.astype(jnp.bfloat16), gating.astype(jnp.bfloat16), squares.astype(jnp.bfloat16)),
        "kv",
        0,
        1,
    )
    inverse_rms = lax.rsqrt(squares / MODEL + EPS)[:, None]
    projected = (projected * inverse_rms).reshape(seqs_here, 4, heads_here, head_width)
    gating = gating * inverse_rms
    queries = projected[:, 0]
    key_raw = projected[:, 1]
    key_new = (key_raw * lax.rsqrt(jnp.sum(key_raw * key_raw, axis=2, keepdims=True) + EPS)).astype(
        jnp.bfloat16
    )
    value_new = projected[:, 2].astype(jnp.bfloat16)
    gate_raw = projected[:, 3]
    beta_new = jax.nn.sigmoid(gating[:, :heads_here])
    decay_new = -decay_rate * jax.nn.softplus(gating[:, heads_here:])
    readout, new_state = delta_block(
        queries,
        key_new,
        value_new,
        beta_new,
        decay_new,
        block_keys,
        block_values,
        block_beta,
        block_decay,
        live_count,
        carried_state,
    )
    scaled = (
        readout * lax.rsqrt(jnp.mean(readout * readout, axis=2, keepdims=True) + EPS) * head_gain
    )
    mixed_heads = (
        (scaled * jax.nn.silu(gate_raw))
        .reshape(seqs_here, heads_here * head_width)
        .astype(jnp.bfloat16)
    )
    attended = jnp.dot(
        collect(mixed_heads, "kv", 0), out_weight, preferred_element_type=jnp.float32
    )
    attended = over_copies(attended.astype(jnp.bfloat16), "tp").astype(jnp.float32)
    residual = lax.optimization_barrier((token_vals + attended).astype(jnp.bfloat16))
    resid_vals = residual.astype(jnp.float32)
    mlp_squares = jnp.sum(resid_vals * resid_vals, axis=1)
    gain_part = lax.dynamic_slice_in_dim(mlp_gain, kv_index * columns, columns, 0)
    mlp_in = (resid_vals * gain_part).astype(jnp.bfloat16)
    pre_act = jnp.dot(mlp_in, up_weight, preferred_element_type=jnp.float32)
    pre_act, mlp_squares = side_by_side(
        (pre_act.astype(jnp.bfloat16), mlp_squares.astype(jnp.bfloat16)), "kv", 0, 1
    )
    hidden = jnp.square(
        jax.nn.relu(pre_act * lax.rsqrt(mlp_squares / MODEL + EPS)[:, None])
    ).astype(jnp.bfloat16)
    output_part = jnp.dot(collect(hidden, "kv", 0), down_weight, preferred_element_type=jnp.float32)
    output_part = over_copies(output_part.astype(jnp.bfloat16), "tp").astype(jnp.float32)
    mixed = (resid_vals + output_part).astype(jnp.bfloat16)
    return (mixed, new_state)


def solution(mesh):
    placed = (
        P(None, "kv"),
        P("kv"),
        P("kv", "tp"),
        P("kv", "tp"),
        P("kv", "tp"),
        P("kv", "tp"),
        P(),
        P(),
        P("tp"),
        P(),
        P("kv", "tp", None, None),
        P("kv", "tp", None, None),
        P("kv", "tp", None, None),
        P("kv", "tp", None),
        P("kv", "tp", None),
        P("kv"),
        P("tp", "kv"),
        P(),
        P("kv", "tp"),
        P("tp", "kv"),
    )
    return jax.shard_map(
        body,
        mesh=mesh,
        in_specs=placed,
        out_specs=(P(None, "kv"), P("kv", "tp", None, None)),
        check_vma=False,
    )
```

profile of v0, /device:TPU:1, one launch (start us, length us, event | category | flops | bytes accessed | tf_op | source)
XLA Modules:
  0.0 136.4 jit_solution(1740215875416192299)
XLA Ops:
  0.7 0.8 dynamic_slice.9
  1.4 0.8 dynamic_slice.10
  2.2 0.8 fusion.36
  3.0 1.0 convolution_convert_fusion.4
  4.3 1.2 fusion
  5.6 1.0 concatenate.24
  6.6 12.0 %all-to-all-start = ((bf16[32,8,1029]{2,1,0:T(8,128)(2,1)}), bf16[32,8,1029]{2,1,0:T(8,128)(2,1)S(1)}, u32[]{:S(2)}, u32[]{:S(2)}) async-start(bf16[32,8,1029]{2,1,0:T(8,128)(2,1)} %concatenate.24), calls=%async_computation | async-start | bytes 1179648 | tf_op jit(solution)/shard_map/all_to_all | solution.py:21
  18.7 17.4 %all-to-all-done = bf16[32,8,1029]{2,1,0:T(8,128)(2,1)S(1)} async-done(((bf16[32,8,1029]{2,1,0:T(8,128)(2,1)}), bf16[32,8,1029]{2,1,0:T(8,128)(2,1)S(1)}, u32[]{:S(2)}, u32[]{:S(2)}) %all-to-all-start) | async-done | bytes 526880 | tf_op jit(solution)/shard_map/all_to_all | solution.py:21
  39.2 0.6 fusion.74
  39.8 0.7 convolution_add_fusion.5
  41.8 0.6 fusion.76
  45.1 0.9 fusion.5
  46.0 0.9 fusion.7
  46.9 1.1 convolution_subtract_fusion
  48.0 2.3 %convolution_add_fusion = f32[8,2,128,128]{3,2,1,0:T(8,128)S(1)} fusion(f32[8,2,64,128]{3,2,1,0:T(8,128)S(1)} %convolution_subtract_fusion, f32[8,2,128,128]{3,2,1,0:T(8,128)S(1)} %copy-done.1, f32[8,2]{1,0:T(8,128)S(1)} %copy.98, f32[8,2,64]{2,1,0:T(2,128)S(1)} %copy.100, bf16[8,2,64,128]{3,2,1,0:T(8,128)(2,1)S(1)} %copy-done.3, ...), kind=kOutput, calls=%fused_computation | convolution fusion | flops 202375168 | bytes 2892864 | tf_op jit(solution)/shard_map/shik,shiv->shkv/dot_general | solution.py:114
  50.4 1.0 fusion.53
  51.6 14.5 %all_to_all.30 = bf16[32,8,256]{2,1,0:T(8,128)(2,1)S(1)} all-to-all(bf16[32,8,256]{2,1,0:T(8,128)(2,1)S(1)} %broadcast_in_dim.139), channel_id=1, replica_groups=mesh['kv'=32,'tp'=8] {'kv'}, dimensions={0} | all-to-all | bytes 262144 | tf_op jit(solution)/shard_map/all_to_all | solution.py:44
  66.2 0.7 broadcast_in_dim.140
  67.0 7.5 %all-to-all-start.2 = ((bf16[8,256,64]{1,2,0:T(8,128)(2,1)}), bf16[8,256,64]{1,2,0:T(8,128)(2,1)S(1)}, u32[]{:S(2)}, u32[]{:S(2)}) async-start(bf16[8,256,64]{1,2,0:T(8,128)(2,1)} %broadcast_in_dim.140), calls=%async_computation.2 | async-start | bytes 524288 | tf_op jit(solution)/shard_map/all_to_all | solution.py:44
  74.5 0.8 dynamic_slice.11
  75.3 5.7 %all-to-all-done.2 = bf16[8,256,64]{1,2,0:T(8,128)(2,1)S(1)} async-done(((bf16[8,256,64]{1,2,0:T(8,128)(2,1)}), bf16[8,256,64]{1,2,0:T(8,128)(2,1)S(1)}, u32[]{:S(2)}, u32[]{:S(2)}) %all-to-all-start.2) | async-done | bytes 262176 | tf_op jit(solution)/shard_map/all_to_all | solution.py:44
  81.8 19.9 %all_to_all.31 = bf16[32,8,1025]{2,1,0:T(8,128)(2,1)S(1)} all-to-all(bf16[32,8,1025]{2,1,0:T(8,128)(2,1)S(1)} %pad_maximum_fusion), channel_id=1, replica_groups=mesh['kv'=32,'tp'=8] {'kv'}, dimensions={0} | all-to-all | bytes 1049600 | tf_op jit(solution)/shard_map/all_to_all | solution.py:21
  102.1 20.8 %all_to_all.32 = bf16[32,8,1024]{2,1,0:T(8,128)(2,1)S(1)} all-to-all(bf16[32,8,1024]{2,1,0:T(8,128)(2,1)S(1)} %broadcast_in_dim.141), channel_id=1, replica_groups=mesh['kv'=32,'tp'=8] {'kv'}, dimensions={0} | all-to-all | bytes 1048576 | tf_op jit(solution)/shard_map/all_to_all | solution.py:44
  123.2 12.6 %all_to_all.33 = bf16[8,256,64]{1,2,0:T(8,128)(2,1)S(1)} all-to-all(bf16[8,256,64]{1,2,0:T(8,128)(2,1)S(1)} %broadcast_in_dim.142), channel_id=1, replica_groups=mesh['kv'=32,'tp'=8] {'tp'}, dimensions={0} | all-to-all | bytes 524288 | tf_op jit(solution)/shard_map/all_to_all | solution.py:44
  (84 shorter events, 9.9 us)
Async XLA Ops:
  0.6 80.7 %copy-start = (bf16[64,1024]{1,0:T(8,128)(2,1)S(1)}, bf16[64,1024]{1,0:T(8,128)(2,1)}, u32[]{:S(2)}) copy-start(bf16[64,1024]{1,0:T(8,128)(2,1)} %param.38) | copy-start | bytes 393220
  5.6 13.0 %copy-start.11 = (f32[2]{0:T(128)S(1)}, f32[2]{0:T(128)}, u32[]{:S(2)}) copy-start(f32[2]{0:T(128)} %param.28) | copy-start | bytes 28
  5.6 13.0 %copy-start.12 = (s32[8]{0:T(128)S(1)}, s32[8]{0:T(128)}, u32[]{:S(2)}) copy-start(s32[8]{0:T(128)} %param.35) | copy-start | bytes 100
  6.6 30.2 %copy-start.8 = (f32[8,2,64]{2,1,0:T(2,128)S(1)}, f32[8,2,64]{2,1,0:T(2,128)}, u32[]{:S(2)}) copy-start(f32[8,2,64]{2,1,0:T(2,128)} %param.34) | copy-start | bytes 12292
  6.6 31.2 %copy-start.9 = (f32[8,2,64]{2,1,0:T(2,128)S(1)}, f32[8,2,64]{2,1,0:T(2,128)}, u32[]{:S(2)}) copy-start(f32[8,2,64]{2,1,0:T(2,128)} %param.33) | copy-start | bytes 12292
  6.6 31.3 %copy-start.3 = (bf16[8,2,64,128]{3,2,1,0:T(8,128)(2,1)S(1)}, bf16[8,2,64,128]{3,2,1,0:T(8,128)(2,1)}, u32[]{:S(2)}) copy-start(bf16[8,2,64,128]{3,2,1,0:T(8,128)(2,1)} %param.31) | copy-start | bytes 786436
  6.6 29.5 %all-to-all-start = ((bf16[32,8,1029]{2,1,0:T(8,128)(2,1)}), bf16[32,8,1029]{2,1,0:T(8,128)(2,1)S(1)}, u32[]{:S(2)}, u32[]{:S(2)}) async-start(bf16[32,8,1029]{2,1,0:T(8,128)(2,1)} %concatenate.24), calls=%async_computation | async-start | bytes 1179648 | tf_op jit(solution)/shard_map/all_to_all | solution.py:21
  45.1 1.0 copy-start.5
  45.1 1.8 %copy-start.1 = (f32[8,2,128,128]{3,2,1,0:T(8,128)S(1)}, f32[8,2,128,128]{3,2,1,0:T(8,128)}, u32[]{:S(2)}) copy-start(f32[8,2,128,128]{3,2,1,0:T(8,128)} %param.30) | copy-start | bytes 3145732
  50.3 16.6 %copy-start.2 = (f32[8,2,128,128]{3,2,1,0:T(8,128)}, f32[8,2,128,128]{3,2,1,0:T(8,128)S(1)}, u32[]{:S(2)}) copy-start(f32[8,2,128,128]{3,2,1,0:T(8,128)S(1)} %convolution_add_fusion) | copy-start | bytes 3145732
  50.4 1.1 copy-start.10
  50.4 15.7 %copy-start.7 = (bf16[256,64]{0,1:T(8,128)(2,1)S(1)}, bf16[256,64]{0,1:T(8,128)(2,1)}, u32[]{:S(2)}) copy-start(bf16[256,64]{0,1:T(8,128)(2,1)} %param.36) | copy-start | bytes 98308
  51.4 29.7 %copy-start.4 = (bf16[256,64]{0,1:T(8,128)(2,1)S(1)}, bf16[256,64]{0,1:T(8,128)(2,1)}, u32[]{:S(2)}) copy-start(bf16[256,64]{0,1:T(8,128)(2,1)} %param.20) | copy-start | bytes 98308
  67.0 14.0 %all-to-all-start.2 = ((bf16[8,256,64]{1,2,0:T(8,128)(2,1)}), bf16[8,256,64]{1,2,0:T(8,128)(2,1)S(1)}, u32[]{:S(2)}, u32[]{:S(2)}) async-start(bf16[8,256,64]{1,2,0:T(8,128)(2,1)} %broadcast_in_dim.140), calls=%async_computation.2 | async-start | bytes 524288 | tf_op jit(solution)/shard_map/all_to_all | solution.py:44
  101.7 21.2 %copy-start.6 = (bf16[1024,64]{0,1:T(8,128)(2,1)S(1)}, bf16[1024,64]{0,1:T(8,128)(2,1)}, u32[]{:S(2)}) copy-start(bf16[1024,64]{0,1:T(8,128)(2,1)} %param.39) | copy-start | bytes 393220
where the time goes:
time: 137 us; the launch traced here: 136 us
  blocking collectives  67.8 us (49%)
  waiting for transfers between devices  23.1 us (17%)
  starting transfers between devices  19.5 us (14%)
  matrix products  16.2 us (12%)
  local copies, waits for them, and re-layouts  5.31 us (4%)
  other arithmetic  3.41 us (2%)
    all_to_all x3, blocking collectives, sent_to_all(): return lax.all_to_all(copies, axis, split_axis=0, concat_axis=0, tiled=True)  47.9 us
    all_to_all x1, blocking collectives, sent_and_summed(): tiles = lax.all_to_all(in_blocks(x, dim, devices), axis, 0, 0, tiled=True)  19.9 us
    all_to_all x1, waiting for transfers between devices, sent_and_summed(): tiles = lax.all_to_all(in_blocks(x, dim, devices), axis, 0, 0, tiled=True)  17.4 us
    all_to_all x1, starting transfers between devices, sent_and_summed(): tiles = lax.all_to_all(in_blocks(x, dim, devices), axis, 0, 0, tiled=True)  12 us
    all_to_all x1, starting transfers between devices, sent_to_all(): return lax.all_to_all(copies, axis, split_axis=0, concat_axis=0, tiled=True)  7.53 us
    all_to_all x1, waiting for transfers between devices, sent_to_all(): return lax.all_to_all(copies, axis, split_axis=0, concat_axis=0, tiled=True)  5.71 us
    dot_general x5, matrix products, unit_inverse(): jnp.matmul(product_sum, powered, precision=PRECISE)  3.24 us
    dot_general x5, matrix products, unit_inverse(): powered = jnp.matmul(powered, powered, precision=PRECISE)  3.22 us
  transfers between devices with their start and end apart: 2, of which 2 were waited for; matrix products, arithmetic and copies ran while one was open for 1% of the time, Pallas kernels for 0%

commit v1 on v0

v1 whole, which is shorter than its diff:
```python
import functools

import jax
import jax.numpy as jnp
from jax import lax
from jax.experimental import pallas as pl
from jax.experimental.pallas import tpu as pltpu
from jax.sharding import PartitionSpec as P

MODEL = 2048
HEADS = 16
EPS = 1e-06
NX = 4
F32 = jnp.float32
BF16 = jnp.bfloat16


def dot(a, b):
    return jnp.dot(a, b, preferred_element_type=F32)


def split(a):
    high = a.astype(BF16)
    return high, (a - high.astype(F32)).astype(BF16)


def dot3(a, b):
    ah, al = split(a)
    bh, bl = split(b)
    return dot(ah, bh) + (dot(ah, bl) + dot(al, bh))


def dot2(a, b):
    bh, bl = split(b)
    return dot(a, bh) + dot(a, bl)


def iota(shape, dim):
    return lax.broadcasted_iota(jnp.int32, shape, dim)


def unit_inverse(lower, r, c):
    def same(bits):
        return (r >> bits) == (c >> bits)

    ident = jnp.where(r == c, 1.0, 0.0)
    power = jnp.where(same(3), -lower, 0.0)
    total = ident + power
    for _ in range(2):
        power = dot3(power, power)
        total = total + dot3(total, power)
    for bits in (3, 4, 5):
        off = jnp.where(same(bits + 1) & jnp.logical_not(same(bits)), lower, 0.0)
        total = total - dot3(total, dot3(off, total))
    return total


def state_before(g, keys, vals, state, bbeta, bdecay, live):
    r = iota((256, 256), 0)
    c = iota((256, 256), 1)
    same = (r >> 6) == (c >> 6)
    n0, n1 = live[2 * g] - 1, live[2 * g + 1] - 1
    lane = iota((1, 256), 1)
    live_row = (lane & 63) < jnp.where(lane < 128, n0, n1)
    d_row = jnp.where(live_row, bdecay[g], 0.0)
    b_row = jnp.where(live_row, bbeta[g], 0.0)
    r1 = iota((256, 128), 0)
    live_col = (r1 & 63) < jnp.where(r1 < 128, n0, n1)
    k_all = jnp.where(live_col, keys[pl.ds(2 * g, 2)].astype(F32).reshape(256, 128), 0.0)
    v_all = jnp.where(live_col, vals[pl.ds(2 * g, 2)].astype(F32).reshape(256, 128), 0.0)
    d_col = jnp.sum(jnp.where(r == c, d_row, 0.0), axis=1, keepdims=True)
    b_col = jnp.sum(jnp.where(r == c, b_row, 0.0), axis=1, keepdims=True)
    tot_col = jnp.sum(jnp.where(same & (c <= r), d_row, 0.0), axis=1, keepdims=True)
    tot_row = jnp.sum(jnp.where(same & (r <= c), d_col, 0.0), axis=0, keepdims=True)
    end_col = jnp.sum(jnp.where(same, d_row, 0.0), axis=1, keepdims=True)
    kb = k_all.astype(BF16)
    kt = k_all.T.astype(BF16)
    strict = same & (c < r)
    fade = jnp.exp(jnp.where(strict, tot_col - tot_row, 0.0))
    lower = jnp.where(strict, b_col * dot(kb, kt) * fade, 0.0)
    inverse = unit_inverse(lower, r, c)
    old = jnp.concatenate([state[2 * g + p // 2, p % 2] for p in range(4)], axis=1)
    seen = dot2(kb, old)
    seen = jnp.concatenate(
        [seen[64 * p : 64 * p + 64, 128 * p : 128 * p + 128] for p in range(4)], axis=0
    )
    right = b_col * (v_all - jnp.exp(tot_col) * seen)
    update = dot3(inverse, right) * jnp.exp(end_col - tot_col)
    r4 = iota((256, 512), 0)
    c4 = iota((256, 512), 1)
    wide = jnp.concatenate([update] * 4, axis=1)
    wide = jnp.where((r4 >> 6) == (c4 >> 7), wide, 0.0)
    added = dot2(kt, wide)
    for p in range(4):
        end = jnp.exp(end_col[64 * p : 64 * p + 1, :])
        at = slice(128 * p, 128 * p + 128)
        state[2 * g + p // 2, p % 2] = end * old[:, at] + added[:, at]


def halves(a):
    n = a.shape[0] // 2
    return jnp.concatenate([a[:n], a[n:]], axis=1)


def folded(a, blocks):
    n = a.shape[0] // 2
    return [
        a[:n, 128 * b : 128 * b + 64] + a[n:, 128 * b + 64 : 128 * b + 128] for b in range(blocks)
    ]


def kernel(
    tok_ref,
    ngain_ref,
    qw_hbm,
    kw_hbm,
    vw_hbm,
    gw_hbm,
    bw_hbm,
    dw_hbm,
    rate_ref,
    hgain_ref,
    state_hbm,
    keys_hbm,
    vals_hbm,
    bbeta_ref,
    bdecay_ref,
    live_ref,
    out_hbm,
    mgain_ref,
    up_hbm,
    down_hbm,
    mixed_ref,
    nstate_hbm,
    wst,
    wcat,
    bwv,
    dwv,
    tokp,
    gp,
    tokt,
    proj_s,
    proj_r,
    ex_s,
    ex_r,
    keys,
    vals,
    state,
    up_all,
    down_all,
    out_all,
    down_tmp,
    out_tmp,
    bbeta,
    bdecay,
    mh,
    ar,
    ax,
    rs_s,
    rs_r,
    resid,
    fin_s,
    mx,
    loc,
    xs,
    xr,
    ts,
    tr,
    ps,
    pr,
    ms,
    mr,
    asem,
    arr,
    us,
    ur,
    ds_,
    dr,
    fs,
    fr,
    ring_s,
    ring_r,
    *,
    n_kv,
    n_tp,
):
    kv = lax.axis_index("kv")
    tp = lax.axis_index("tp")
    nz = n_kv // NX
    z = kv // NX
    x = kv % NX

    def local(src, dst, i):
        copy = pltpu.make_async_copy(src, dst, loc.at[i])
        copy.start()
        return copy

    def remote(src, dst, s, r, kv_to, tp_to):
        return pltpu.make_async_remote_copy(
            src_ref=src,
            dst_ref=dst,
            send_sem=s,
            recv_sem=r,
            device_id={"kv": kv_to, "tp": tp_to},
            device_id_type=pl.DeviceIdType.MESH,
        )

    in_w = [local(w, wst.at[i], i) for i, w in enumerate((qw_hbm, kw_hbm, vw_hbm, gw_hbm))]
    rows = pl.ds(pl.multiple_of(z * 256, 256), 256)
    in_b = [local(bw_hbm.at[rows], bwv, 4), local(dw_hbm.at[rows], dwv, 5)]
    in_out = local(out_hbm, out_tmp, 6)
    in_up = local(up_hbm, up_all.at[z], 7)
    in_down = local(down_hbm, down_tmp, 8)
    in_keys = local(keys_hbm, keys, 9)
    in_vals = local(vals_hbm, vals, 10)
    in_state = local(state_hbm, state, 11)

    barrier = pltpu.get_barrier_semaphore()

    def greet_kv(d, carry):
        pl.semaphore_signal(
            barrier,
            inc=1,
            device_id={"kv": (kv + d) % n_kv, "tp": tp},
            device_id_type=pl.DeviceIdType.MESH,
        )
        return carry

    def greet_tp(d, carry):
        pl.semaphore_signal(
            barrier,
            inc=1,
            device_id={"kv": kv, "tp": (tp + d) % n_tp},
            device_id_type=pl.DeviceIdType.MESH,
        )
        return carry

    lax.fori_loop(1, n_kv, greet_kv, 0)
    lax.fori_loop(1, n_tp, greet_tp, 0)

    tokp[x] = halves(tok_ref[...].astype(F32)).astype(BF16)
    gp[x] = jnp.concatenate([ngain_ref[...], ngain_ref[...]], axis=1)
    for i in range(4):
        bbeta[i] = jnp.concatenate([bbeta_ref[2 * i + j // 2, j % 2 : j % 2 + 1] for j in range(4)], axis=1)
        bdecay[i] = jnp.concatenate([bdecay_ref[2 * i + j // 2, j % 2 : j % 2 + 1] for j in range(4)], axis=1)
    for copy in in_b:
        copy.wait()
    wcat[:, 256:384] = jnp.concatenate(
        [bwv[...].astype(F32), dwv[...].astype(F32), jnp.zeros((256, 96), F32)], axis=1
    ).astype(BF16)
    for copy in in_w:
        copy.wait()
    wcat[pl.ds(pl.multiple_of(x * 64, 64), 64), 0:256] = wst[x]
    in_out.wait()
    lane_z = pl.ds(pl.multiple_of(z * 128, 128), 128)
    out_all[:, lane_z] = halves(out_tmp[...].astype(F32)).astype(BF16)
    in_up.wait()
    in_down.wait()
    down_all[:, lane_z] = halves(down_tmp[...].astype(F32)).astype(BF16)
    tokt[z] = tok_ref[pl.ds(pl.multiple_of(z * 32, 32), 32), :]

    pl.semaphore_wait(barrier, n_kv - 1 + n_tp - 1)

    mine = pl.ds(pl.multiple_of(x * 64, 64), 64)
    sent_x = []
    for d in range(1, NX):
        to = (x + d) % NX
        peer = z * NX + to
        sent_x.append(remote(tokp.at[x], tokp.at[x], xs.at[0, d], xr.at[0, d], peer, tp))
        sent_x.append(remote(gp.at[x], gp.at[x], xs.at[1, d], xr.at[1, d], peer, tp))
        sent_x.append(
            remote(wst.at[to], wcat.at[mine, pl.ds(0, 256)], xs.at[2, d], xr.at[2, d], peer, tp)
        )
    for copy in sent_x:
        copy.start()

    sent_t = []
    for d in range(1, nz):
        to = (z + d) % nz
        sent_t.append(
            remote(
                tok_ref.at[pl.ds(pl.multiple_of(to * 32, 32), 32), :],
                tokt.at[z],
                ts.at[d],
                tr.at[d],
                to * NX + x,
                tp,
            )
        )
    for copy in sent_t:
        copy.start()

    def ring(way, step, what):
        to = (z + 1) % nz if way == 0 else (z + nz - 1) % nz
        block = (z + nz - (step - 1)) % nz if way == 0 else (z + step - 1) % nz
        lanes = pl.ds(pl.multiple_of(block * 128, 128), 128)
        ref = (out_all.at[:, lanes], up_all.at[block], down_all.at[:, lanes])[what]
        return remote(
            ref, ref, ring_s.at[way, step - 1, what], ring_r.at[way, step - 1, what], to * NX + x, tp
        )

    half = nz // 2
    plan = {}
    for step in range(1, half + 1):
        plan[step] = [
            (way, what)
            for what in range(3)
            for way in range(2)
            if step < half or way == (1 if what == 2 else 0)
        ]

    def ring_start(step):
        for way, what in plan[step]:
            ring(way, step, what).start()

    def ring_pass(step):
        for way, what in plan[step]:
            ring(way, step, what).wait_recv()
            if step < half and (way, what) in plan[step + 1]:
                ring(way, step + 1, what).start()

    ring_start(1)

    in_keys.wait()
    in_vals.wait()
    in_state.wait()

    def before(g, carry):
        state_before(g, keys, vals, state, bbeta, bdecay, live_ref)
        return carry

    lax.fori_loop(0, 2, before, 0)

    for copy in sent_x:
        copy.wait_recv()
    parts, squares = [], jnp.zeros((128, 128), F32)
    for i in range(NX):
        t = tokp[i].astype(F32)
        squares = squares + t * t
        parts.append(t * gp[i])
    tops = jnp.concatenate([p[:, :64] for p in parts], axis=1)
    bottoms = jnp.concatenate([p[:, 64:] for p in parts], axis=1)
    normed = jnp.concatenate([tops, bottoms], axis=0).astype(BF16)
    squares = jnp.concatenate(
        [
            jnp.sum(squares[:, :64], axis=1, keepdims=True),
            jnp.sum(squares[:, 64:], axis=1, keepdims=True),
        ],
        axis=0,
    )
    projected = dot(normed, wcat[...])
    proj_s[...] = projected[:, :256].reshape(n_kv, 8, 256).astype(BF16)
    lane = iota((256, 128), 1)
    high = squares.astype(BF16).astype(F32)
    extra = projected[:, 256:384]
    extra = jnp.where(lane == 32, high, jnp.where(lane == 33, squares - high, extra))
    ex_s[...] = extra.reshape(n_kv, 8, 128).astype(BF16)
    proj_r[kv] = proj_s[kv]
    ex_r[z] = ex_s[kv]

    def send_proj(d, carry):
        to = (kv + d) % n_kv
        remote(proj_s.at[to], proj_r.at[kv], ps.at[0], pr.at[0], to, tp).start()
        return carry

    def send_extra(d, carry):
        to = ((z + d) % nz) * NX + x
        remote(ex_s.at[to], ex_r.at[z], ps.at[1], pr.at[1], to, tp).start()
        return carry

    lax.fori_loop(1, nz, send_extra, 0)
    lax.fori_loop(1, n_kv, send_proj, 0)

    ring_pass(1)
    lax.fori_loop(2, 4, before, 0)

    some = pl.ds(0, n_kv - 1)
    few = pl.ds(0, nz - 1)
    all_proj = remote(proj_s.at[some], proj_r.at[some], ps.at[0], pr.at[0], kv, tp)
    all_extra = remote(ex_s.at[few], ex_r.at[few], ps.at[1], pr.at[1], kv, tp)
    all_extra.wait_recv()
    all_proj.wait_recv()

    total = jnp.sum(proj_r[...].astype(F32).reshape(nz, NX, 8, 256), axis=0)
    extra = jnp.sum(ex_r[...].astype(F32), axis=0)
    inverse_rms = lax.rsqrt((extra[:, 32:33] + extra[:, 33:34]) / MODEL + EPS)
    extra = extra * inverse_rms
    queries, key_raw, value_raw, gate_raw = [total[i] * inverse_rms for i in range(4)]
    lane = iota((8, 128), 1)
    cols, heads = [], []
    for h in range(2):
        at = slice(128 * h, 128 * h + 128)
        k = key_raw[:, at]
        k = k * lax.rsqrt(jnp.sum(k * k, axis=1, keepdims=True) + EPS)
        k = k.astype(BF16).astype(F32)
        v = value_raw[:, at].astype(BF16).astype(F32)
        q = queries[:, at]
        b = jnp.sum(jnp.where(lane == 2 * tp + h, extra, 0.0), axis=1, keepdims=True)
        b = 1.0 / (1.0 + jnp.exp(-b))
        a = jnp.sum(jnp.where(lane == HEADS + 2 * tp + h, extra, 0.0), axis=1, keepdims=True)
        a = jnp.maximum(a, 0.0) + jnp.log1p(jnp.exp(-jnp.abs(a)))
        e = jnp.exp(-rate_ref[h] * a)
        qk = jnp.sum(q * k, axis=1, keepdims=True)
        cols += [k, q]
        heads.append((k, v, q, b, e, qk))
    columns = jnp.concatenate(cols + [jnp.zeros((96, 128), F32)], axis=0).T
    updates, readouts = {}, []
    for h in range(2):
        k, v, q, b, e, qk = heads[h]
        lines = []
        for s in range(8):
            old = state[s, h]
            one = slice(s, s + 1)
            kcol = columns[:, 16 * h + s : 16 * h + s + 1]
            qcol = columns[:, 16 * h + 8 + s : 16 * h + 9 + s]
            ks = jnp.sum(old * kcol, axis=0, keepdims=True)
            qs = jnp.sum(old * qcol, axis=0, keepdims=True)
            u = b[one] * (v[one] - e[one] * ks)
            updates[s, h] = u
            lines.append(e[one] * qs + qk[one] * u)
        readouts.append(jnp.concatenate(lines, axis=0))
    gated = []
    for h in range(2):
        rd = readouts[h]
        gate = gate_raw[:, 128 * h : 128 * h + 128]
        scaled = rd * lax.rsqrt(jnp.sum(rd * rd, axis=1, keepdims=True) / 128 + EPS) * hgain_ref[...]
        gated.append(scaled * (gate / (1.0 + jnp.exp(-gate))))
    mh[x] = jnp.concatenate(gated, axis=1).astype(BF16).astype(F32)
    sent_m = []
    for d in range(1, NX):
        peer = z * NX + (x + d) % NX
        sent_m.append(remote(mh.at[x], mh.at[x], ms.at[d], mr.at[d], peer, tp))
    for copy in sent_m:
        copy.start()
    ring_pass(2)

    for h in range(2):
        e = heads[h][4]
        for s in range(8):
            kcol = columns[:, 16 * h + s : 16 * h + s + 1]
            state[s, h] = e[s : s + 1] * state[s, h] + kcol * updates[s, h]
    put_state = local(state, nstate_hbm, 0)
    ring_pass(3)

    for copy in sent_m:
        copy.wait_recv()
    ring_pass(4)
    m = mh[...].reshape(32, 256)
    m = jnp.concatenate([m[:, :128], m[:, 128:]], axis=0).astype(BF16)
    blocks = folded(dot(m, out_all[...]), nz)
    ar[tp] = jnp.concatenate(blocks, axis=1).astype(BF16)

    def send_ar(d, carry):
        to = (tp + d) % n_tp
        remote(ar.at[tp], ar.at[tp], asem, arr, kv, to).start()
        return carry

    lax.fori_loop(1, n_tp, send_ar, 0)
    tps = pl.ds(0, n_tp - 1)
    all_ar = remote(ar.at[tps], ar.at[tps], asem, arr, kv, tp)
    for copy in sent_t:
        copy.wait_recv()
    tokens = jnp.concatenate([tokt[i].astype(F32) for i in range(nz)], axis=1)
    gains = []
    for p in range(nz):
        gain = mgain_ref[pl.ds(2 * p + x // 2, 1), :]
        gains.append(jnp.where(x % 2 == 0, gain[:, :64], gain[:, 64:]))
    gains = jnp.concatenate(gains, axis=1)
    all_ar.wait_recv()

    attended = jnp.sum(ar[...].astype(F32), axis=0)
    residual = (tokens + attended).astype(BF16).astype(F32)
    for i in range(nz):
        resid[i] = residual[:, 64 * i : 64 * i + 64]
    squares = jnp.sum(residual * residual, axis=1, keepdims=True)
    mlp_in = (residual * gains).astype(BF16)
    pre = dot(mlp_in, up_all[...].reshape(nz * 64, 1024))
    high = squares.astype(BF16).astype(F32)
    lane = iota((32, 128), 1)
    tail = jnp.where(lane == 0, high, jnp.where(lane == 1, squares - high, 0.0))
    ax[x] = jnp.concatenate([pre, tail], axis=1).astype(BF16)
    sent_u = []
    for d in range(1, NX):
        peer = z * NX + (x + d) % NX
        sent_u.append(remote(ax.at[x], ax.at[x], us.at[d], ur.at[d], peer, tp))
    for copy in sent_u:
        copy.start()
    for copy in sent_u:
        copy.wait_recv()
    total = jnp.sum(ax[...].astype(F32), axis=0)
    rms = lax.rsqrt((total[:, 1024:1025] + total[:, 1025:1026]) / MODEL + EPS)
    hidden = jnp.maximum(total[:, :1024] * rms, 0.0)
    hidden = (hidden * hidden).astype(BF16)
    hidden = jnp.concatenate([hidden[:, :512], hidden[:, 512:]], axis=0)
    blocks = folded(dot(hidden, down_all[...]), nz)
    for i in range(nz):
        rs_s[i] = blocks[i].astype(BF16)
    rs_r[tp] = rs_s[tp]

    def send_rs(d, carry):
        to = (tp + d) % n_tp
        remote(rs_s.at[to], rs_r.at[tp], ds_, dr, kv, to).start()
        return carry

    lax.fori_loop(1, n_tp, send_rs, 0)
    all_rs = remote(rs_s.at[tps], rs_r.at[tps], ds_, dr, kv, tp)
    all_rs.wait_recv()
    fin_s[...] = (resid[tp] + jnp.sum(rs_r[...].astype(F32), axis=0)).astype(BF16)

    at_home = z == tp
    far = tp * NX + x

    def send_fin(t, carry):
        @pl.when(jnp.logical_or(jnp.logical_not(at_home), t != tp))
        def _():
            remote(fin_s, mx.at[z], fs, fr, far, t).start()

        return carry

    @pl.when(at_home)
    def _():
        mx[z] = fin_s[...]

    lax.fori_loop(0, n_tp, send_fin, 0)

    put_state.wait()
    for copy in sent_x + sent_t + sent_m + sent_u:
        copy.wait_send()
    for step in plan:
        for way, what in plan[step]:
            ring(way, step, what).wait_send()
    all_proj.wait_send()
    all_extra.wait_send()
    all_ar.wait_send()
    all_rs.wait_send()

    eight = remote(mx, mx, fs, fr, kv, tp)
    seven = remote(mx.at[few], mx.at[few], fs, fr, kv, tp)

    @pl.when(at_home)
    def _():
        seven.wait_recv()
        seven.wait_send()

    @pl.when(jnp.logical_not(at_home))
    def _():
        eight.wait_recv()
        eight.wait_send()

    for i in range(nz):
        mixed_ref[32 * i : 32 * i + 32, :] = mx[i]


def body(
    tokens,
    norm_gain,
    query_weight,
    key_weight,
    value_weight,
    gate_weight,
    beta_weight,
    decay_weight,
    decay_rate,
    head_gain,
    carried_state,
    block_keys,
    block_values,
    block_beta,
    block_decay,
    live_count,
    out_weight,
    mlp_gain,
    up_weight,
    down_weight,
):
    n_kv = lax.axis_size("kv")
    n_tp = lax.axis_size("tp")
    nz = n_kv // NX
    vmem = pl.BlockSpec(memory_space=pltpu.VMEM)
    smem = pl.BlockSpec(memory_space=pltpu.SMEM)
    hbm = pl.BlockSpec(memory_space=pl.ANY)
    dma = pltpu.SemaphoreType.DMA
    return pl.pallas_call(
        functools.partial(kernel, n_kv=n_kv, n_tp=n_tp),
        out_shape=(
            jax.ShapeDtypeStruct(tokens.shape, BF16),
            jax.ShapeDtypeStruct(carried_state.shape, F32),
        ),
        in_specs=[vmem, vmem, hbm, hbm, hbm, hbm, hbm, hbm, smem, vmem, hbm, hbm, hbm, vmem, vmem, smem, hbm, vmem, hbm, hbm],
        out_specs=(vmem, hbm),
        scratch_shapes=[
            pltpu.VMEM((4, 64, 256), BF16),
            pltpu.VMEM((256, 384), BF16),
            pltpu.VMEM((256, 16), BF16),
            pltpu.VMEM((256, 16), BF16),
            pltpu.VMEM((NX, 128, 128), BF16),
            pltpu.VMEM((NX, 1, 128), F32),
            pltpu.VMEM((nz, 32, 64), BF16),
            pltpu.VMEM((n_kv, 8, 256), BF16),
            pltpu.VMEM((n_kv, 8, 256), BF16),
            pltpu.VMEM((n_kv, 8, 128), BF16),
            pltpu.VMEM((nz, 8, 128), BF16),
            pltpu.VMEM((8, 2, 64, 128), BF16),
            pltpu.VMEM((8, 2, 64, 128), BF16),
            pltpu.VMEM((8, 2, 128, 128), F32),
            pltpu.VMEM((nz, 64, 1024), BF16),
            pltpu.VMEM((512, 128 * nz), BF16),
            pltpu.VMEM((128, 128 * nz), BF16),
            pltpu.VMEM((1024, 64), BF16),
            pltpu.VMEM((256, 64), BF16),
            pltpu.VMEM((4, 1, 256), F32),
            pltpu.VMEM((4, 1, 256), F32),
            pltpu.VMEM((NX, 8, 256), F32),
            pltpu.VMEM((n_tp, 32, 512), BF16),
            pltpu.VMEM((NX, 32, 1152), BF16),
            pltpu.VMEM((n_tp, 32, 64), BF16),
            pltpu.VMEM((n_tp, 32, 64), BF16),
            pltpu.VMEM((nz, 32, 64), F32),
            pltpu.VMEM((32, 64), BF16),
            pltpu.VMEM((nz, 32, 64), BF16),
            dma((12,)),
            dma((3, NX)),
            dma((3, NX)),
            dma((nz,)),
            dma((nz,)),
            dma((2,)),
            dma((2,)),
            dma((NX,)),
            dma((NX,)),
            dma,
            dma,
            dma((NX,)),
            dma((NX,)),
            dma,
            dma,
            dma,
            dma,
            dma((2, 4, 3)),
            dma((2, 4, 3)),
        ],
        compiler_params=pltpu.CompilerParams(
            collective_id=0, has_side_effects=True, vmem_limit_bytes=48 * 1024 * 1024
        ),
        name="layer",
    )(
        tokens,
        norm_gain.reshape(1, -1),
        query_weight,
        key_weight,
        value_weight,
        gate_weight,
        beta_weight,
        decay_weight,
        decay_rate,
        head_gain.reshape(1, -1),
        carried_state,
        block_keys,
        block_values,
        block_beta,
        block_decay,
        live_count,
        out_weight,
        mlp_gain.reshape(-1, 128),
        up_weight,
        down_weight,
    )


def solution(mesh):
    placed = (
        P(None, "kv"),
        P("kv"),
        P("kv", "tp"),
        P("kv", "tp"),
        P("kv", "tp"),
        P("kv", "tp"),
        P(),
        P(),
        P("tp"),
        P(),
        P("kv", "tp", None, None),
        P("kv", "tp", None, None),
        P("kv", "tp", None, None),
        P("kv", "tp", None),
        P("kv", "tp", None),
        P("kv"),
        P("tp", "kv"),
        P(),
        P("kv", "tp"),
        P("tp", "kv"),
    )
    return jax.shard_map(
        body,
        mesh=mesh,
        in_specs=placed,
        out_specs=(P(None, "kv"), P("kv", "tp", None, None)),
        check_vma=False,
    )
```

time: 137 us -> 83.7 us (0.61)
  blocking collectives: 67.8 us -> 0 us
  Pallas kernels: 0 us -> 65.7 us
  waiting for transfers between devices: 23.1 us -> 0 us
  starting transfers between devices: 19.5 us -> 0 us
  matrix products: 16.2 us -> 0 us
  local copies, waits for them, and re-layouts: 5.31 us -> 16.5 us
  other arithmetic: 3.41 us -> 0 us
    all_to_all x4 -> x0, blocking collectives: 67.8 us -> none  [the longest x3 47.9 us: sent_to_all(): return lax.all_to_all(copies, axis, split_axis=0, concat_axis=0, tiled=True)]
    pallas_call x0 -> x1, Pallas kernels: none -> 65.7 us  [body(): pl.pallas_call(functools.partial(kernel, n_kv=n_kv, n_tp=n_tp), out_shape...]
    all_to_all x2 -> x0, waiting for transfers between devices: 23.1 us -> none  [the longest x1 17.4 us: sent_and_summed(): tiles = lax.all_to_all(in_blocks(x, dim, devices), axis, 0, 0, tiled=True)]
    all_to_all x2 -> x0, starting transfers between devices: 19.5 us -> none  [the longest x1 12 us: sent_and_summed(): tiles = lax.all_to_all(in_blocks(x, dim, devices), axis, 0, 0, tiled=True)]
    dot_general x21 -> x0, matrix products: 16.2 us -> none  [the longest x5 3.24 us: unit_inverse(): jnp.matmul(product_sum, powered, precision=PRECISE)]
    unnamed x26 -> x40, local copies, waits for them, and re-layouts: 0.11 us -> 15 us
    dynamic_slice x3 -> x0, local copies, waits for them, and re-layouts: 2.31 us -> none  [the longest x1 0.8 us: body(): lax.dynamic_slice(beta_weight, (kv_index * columns, tp_index * heads_here...]
    pallas_call x0 -> x1, local copies, waits for them, and re-layouts: none -> 1.54 us  [body(): pl.pallas_call(functools.partial(kernel, n_kv=n_kv, n_tp=n_tp), out_shape...]
  transfers between devices with their start and end apart: 2 -> 0, of which waited for: 2 -> 0; matrix products, arithmetic and copies ran while one was open for 1% -> 0% of each run, Pallas kernels for 0% -> 0%
where the time goes in v1:
time: 83.7 us; the launch traced here: 83 us
  Pallas kernels  65.7 us (78%)
  local copies, waits for them, and re-layouts  16.5 us (20%)
    pallas_call x1, Pallas kernels, body(): pl.pallas_call(functools.partial(kernel, n_kv=n_kv, n_tp=n_tp), out_shape...  65.7 us
    unnamed x40, local copies, waits for them, and re-layouts  15 us

profile of v1, /device:TPU:1, one launch (start us, length us, event | category | flops | bytes accessed | tf_op | source)
XLA Modules:
  0.0 83.0 jit_solution(4117078252874103167)
XLA Ops:
  0.7 1.0 %copy.22.tok_ref = bf16[256,64]{1,0:T(8,128)(2,1)S(1)} copy(bf16[256,64]{0,1:T(8,128)(2,1)} %param.20) | data formatting | bytes 65536 | tf_op args[0]
  1.6 0.9 %copy.25.out_hbm = bf16[256,64]{1,0:T(8,128)(2,1)S(1)} copy(bf16[256,64]{0,1:T(8,128)(2,1)} %param.36) | data formatting | bytes 65536 | tf_op args[16]
  2.5 0.2 copy.26.down_hbm
  2.7 1.1 %copy.23.bw_hbm = bf16[2048,16]{1,0:T(8,128)(2,1)S(1)} copy(bf16[2048,16]{0,1:T(8,128)(2,1)} %param.26) | data formatting | bytes 131072 | tf_op args[6]
  3.8 0.0 copy-start.9
  3.8 0.0 copy-start.10
  3.8 1.1 %copy.24.dw_hbm = bf16[2048,16]{1,0:T(8,128)(2,1)S(1)} copy(bf16[2048,16]{0,1:T(8,128)(2,1)} %param.27) | data formatting | bytes 131072 | tf_op args[7]
  5.0 0.0 copy-start.1
  5.0 0.9 %copy-done.1 = bf16[8,2,64,128]{3,2,1,0:T(8,128)(2,1)S(1)} copy-done((bf16[8,2,64,128]{3,2,1,0:T(8,128)(2,1)S(1)}, bf16[8,2,64,128]{3,2,1,0:T(8,128)(2,1)}, u32[]{:S(2)}) %copy-start.1) | copy-done | bytes 262168
  5.9 0.9 %copy-done.2 = bf16[8,2,64,128]{3,2,1,0:T(8,128)(2,1)S(1)} copy-done((bf16[8,2,64,128]{3,2,1,0:T(8,128)(2,1)S(1)}, bf16[8,2,64,128]{3,2,1,0:T(8,128)(2,1)}, u32[]{:S(2)}) %copy-start.2) | copy-done | bytes 262168
  6.9 0.9 %copy-done.3 = bf16[64,1024]{1,0:T(8,128)(2,1)S(1)} copy-done((bf16[64,1024]{1,0:T(8,128)(2,1)S(1)}, bf16[64,1024]{1,0:T(8,128)(2,1)}, u32[]{:S(2)}) %copy-start.3) | copy-done | bytes 131096
  7.8 0.8 copy-done.5
  8.6 0.8 copy-done.6
  9.3 0.8 copy-done.7
  10.1 0.8 copy-done.8
  10.8 0.7 copy-done.11
  11.5 0.7 copy-done.12
  12.2 0.7 copy-done.13
  12.8 0.7 copy-done.14
  13.5 0.7 copy-done.15
  14.2 65.7 %layer.1 = (bf16[256,64]{1,0:T(8,128)(2,1)S(1)}, f32[8,2,128,128]{3,2,1,0:T(8,128)S(1)}) custom-call(bf16[256,64]{1,0:T(8,128)(2,1)S(1)} %copy.22.tok_ref, f32[1,64]{1,0:T(1,128)S(1)} %bitcast.4, bf16[64,256]{1,0:T(8,128)(2,1)S(1)} %copy-done.5, bf16[64,256]{1,0:T(8,128)(2,1)S(1)} %copy-done.6, bf16[64,256]{1,0:T(8,128)(2,1)S(1)} %copy-done.7, ...), custom_call_target="tpu_custom_call" | custom-call | tf_op jit(solution)/shard_map/layer/pallas_call | solution.py:583
  79.8 0.6 copy-done.4
  80.5 1.5 %copy.27 = bf16[256,64]{0,1:T(8,128)(2,1)} copy(bf16[256,64]{1,0:T(8,128)(2,1)} %copy-done.4) | data formatting | bytes 65536 | tf_op jit(solution)/shard_map/layer/pallas_call | solution.py:583
  82.0 1.0 %copy.29 = f32[8,2,128,128]{3,2,1,0:T(8,128)} copy(f32[8,2,128,128]{3,2,1,0:T(8,128)S(1)} %get-tuple-element.7) | data formatting | bytes 2097152
  (18 shorter events, 0.0 us)
Async XLA Ops:
  0.6 1.9 %copy-start.16 = (bf16[1024,64]{0,1:T(8,128)(2,1)S(1)}, bf16[1024,64]{0,1:T(8,128)(2,1)}, u32[]{:S(2)}) copy-start(bf16[1024,64]{0,1:T(8,128)(2,1)} %param.39) | copy-start | bytes 393220
  0.6 4.3 %copy-start = (f32[8,2,128,128]{3,2,1,0:T(8,128)S(1)}, f32[8,2,128,128]{3,2,1,0:T(8,128)}, u32[]{:S(2)}) copy-start(f32[8,2,128,128]{3,2,1,0:T(8,128)} %state_hbm.1) | copy-start | bytes 3145732
  3.8 1.2 %copy-start.9 = (f32[8,2,64]{2,1,0:T(2,128)S(1)}, f32[8,2,64]{2,1,0:T(2,128)}, u32[]{:S(2)}) copy-start(f32[8,2,64]{2,1,0:T(2,128)} %bbeta_ref.1) | copy-start | bytes 12292
  3.8 1.2 %copy-start.10 = (f32[8,2,64]{2,1,0:T(2,128)S(1)}, f32[8,2,64]{2,1,0:T(2,128)}, u32[]{:S(2)}) copy-start(f32[8,2,64]{2,1,0:T(2,128)} %bdecay_ref.1) | copy-start | bytes 12292
  5.0 1.0 %copy-start.1 = (bf16[8,2,64,128]{3,2,1,0:T(8,128)(2,1)S(1)}, bf16[8,2,64,128]{3,2,1,0:T(8,128)(2,1)}, u32[]{:S(2)}) copy-start(bf16[8,2,64,128]{3,2,1,0:T(8,128)(2,1)} %keys_hbm.1) | copy-start | bytes 786436
  5.9 0.9 %copy-start.2 = (bf16[8,2,64,128]{3,2,1,0:T(8,128)(2,1)S(1)}, bf16[8,2,64,128]{3,2,1,0:T(8,128)(2,1)}, u32[]{:S(2)}) copy-start(bf16[8,2,64,128]{3,2,1,0:T(8,128)(2,1)} %vals_hbm.1) | copy-start | bytes 786436
  6.9 0.9 %copy-start.3 = (bf16[64,1024]{1,0:T(8,128)(2,1)S(1)}, bf16[64,1024]{1,0:T(8,128)(2,1)}, u32[]{:S(2)}) copy-start(bf16[64,1024]{1,0:T(8,128)(2,1)} %up_hbm.1) | copy-start | bytes 393220
  7.8 0.8 copy-start.5
  8.6 0.8 copy-start.6
  9.3 0.8 copy-start.7
  10.1 0.8 copy-start.8
  10.8 0.7 copy-start.11
  11.5 0.7 copy-start.12
  12.2 0.7 copy-start.13
  12.8 0.7 copy-start.14
  13.5 0.7 copy-start.15
  79.8 0.6 copy-start.4

commit v2 on v1

--- a/solution.py
+++ b/solution.py
@@ -22,6 +22,10 @@
 def split(a):
     high = a.astype(BF16)
     return high, (a - high.astype(F32)).astype(BF16)
+
+
+def dot_nt(a, b):
+    return lax.dot_general(a, b, (((1,), (1,)), ((), ())), preferred_element_type=F32)
 
 
 def dot3(a, b):
@@ -97,48 +101,42 @@
         state[2 * g + p // 2, p % 2] = end * old[:, at] + added[:, at]
 
 
-def halves(a):
-    n = a.shape[0] // 2
-    return jnp.concatenate([a[:n], a[n:]], axis=1)
-
-
-def folded(a, blocks):
-    n = a.shape[0] // 2
-    return [
-        a[:n, 128 * b : 128 * b + 64] + a[n:, 128 * b + 64 : 128 * b + 128] for b in range(blocks)
-    ]
-
-
 def kernel(
-    tok_ref,
-    ngain_ref,
+    tok_hbm,
+    ngain_hbm,
     qw_hbm,
     kw_hbm,
     vw_hbm,
     gw_hbm,
     bw_hbm,
     dw_hbm,
-    rate_ref,
-    hgain_ref,
+    rate_hbm,
+    hgain_hbm,
     state_hbm,
     keys_hbm,
     vals_hbm,
-    bbeta_ref,
-    bdecay_ref,
-    live_ref,
+    bbeta_hbm,
+    bdecay_hbm,
+    live_hbm,
     out_hbm,
-    mgain_ref,
+    mgain_hbm,
     up_hbm,
     down_hbm,
     mixed_ref,
     nstate_hbm,
     wst,
     wcat,
-    bwv,
-    dwv,
-    tokp,
+    bdw,
+    tokx,
     gp,
+    tokl,
     tokt,
+    rate_ref,
+    hgain_ref,
+    bbeta_ref,
+    bdecay_ref,
+    live_ref,
+    mgain_ref,
     proj_s,
     proj_r,
     ex_s,
@@ -149,8 +147,6 @@
     up_all,
     down_all,
     out_all,
-    down_tmp,
-    out_tmp,
     bbeta,
     bdecay,
     mh,
@@ -205,15 +201,30 @@
             device_id_type=pl.DeviceIdType.MESH,
         )
 
+    in_tok = local(tok_hbm, tokx.at[x], 12)
+    in_gain = local(ngain_hbm, gp.at[x], 13)
     in_w = [local(w, wst.at[i], i) for i, w in enumerate((qw_hbm, kw_hbm, vw_hbm, gw_hbm))]
-    rows = pl.ds(pl.multiple_of(z * 256, 256), 256)
-    in_b = [local(bw_hbm.at[rows], bwv, 4), local(dw_hbm.at[rows], dwv, 5)]
-    in_out = local(out_hbm, out_tmp, 6)
+    in_out = local(out_hbm, out_all.at[z], 6)
     in_up = local(up_hbm, up_all.at[z], 7)
-    in_down = local(down_hbm, down_tmp, 8)
-    in_keys = local(keys_hbm, keys, 9)
-    in_vals = local(vals_hbm, vals, 10)
-    in_state = local(state_hbm, state, 11)
+    in_down = local(down_hbm, down_all.at[z], 8)
+    lanes_z = pl.ds(pl.multiple_of(z * 256, 256), 256)
+    in_b = [
+        local(bw_hbm.at[:, lanes_z], bdw.at[0], 4),
+        local(dw_hbm.at[:, lanes_z], bdw.at[1], 5),
+    ]
+    in_block = [
+        local(bbeta_hbm, bbeta_ref, 14),
+        local(bdecay_hbm, bdecay_ref, 15),
+        local(live_hbm, live_ref, 16),
+        local(keys_hbm, keys, 9),
+        local(vals_hbm, vals, 10),
+        local(state_hbm, state, 11),
+    ]
+    in_small = [
+        local(rate_hbm, rate_ref, 17),
+        local(hgain_hbm, hgain_ref, 18),
+        local(mgain_hbm, mgain_ref, 19),
+    ]
 
     barrier = pltpu.get_barrier_semaphore()
 
@@ -238,38 +249,28 @@
     lax.fori_loop(1, n_kv, greet_kv, 0)
     lax.fori_loop(1, n_tp, greet_tp, 0)
 
-    tokp[x] = halves(tok_ref[...].astype(F32)).astype(BF16)
-    gp[x] = jnp.concatenate([ngain_ref[...], ngain_ref[...]], axis=1)
-    for i in range(4):
-        bbeta[i] = jnp.concatenate([bbeta_ref[2 * i + j // 2, j % 2 : j % 2 + 1] for j in range(4)], axis=1)
-        bdecay[i] = jnp.concatenate([bdecay_ref[2 * i + j // 2, j % 2 : j % 2 + 1] for j in range(4)], axis=1)
-    for copy in in_b:
-        copy.wait()
-    wcat[:, 256:384] = jnp.concatenate(
-        [bwv[...].astype(F32), dwv[...].astype(F32), jnp.zeros((256, 96), F32)], axis=1
-    ).astype(BF16)
+    in_tok.wait()
+    in_gain.wait()
+    tokl[...] = tokx[x].astype(F32).T.astype(BF16)
+    tokt[z] = tokl[pl.ds(pl.multiple_of(z * 32, 32), 32), :]
     for copy in in_w:
         copy.wait()
-    wcat[pl.ds(pl.multiple_of(x * 64, 64), 64), 0:256] = wst[x]
+    mine = pl.ds(pl.multiple_of(x * 64, 64), 64)
+    wcat[mine, :] = wst[x]
     in_out.wait()
-    lane_z = pl.ds(pl.multiple_of(z * 128, 128), 128)
-    out_all[:, lane_z] = halves(out_tmp[...].astype(F32)).astype(BF16)
     in_up.wait()
     in_down.wait()
-    down_all[:, lane_z] = halves(down_tmp[...].astype(F32)).astype(BF16)
-    tokt[z] = tok_ref[pl.ds(pl.multiple_of(z * 32, 32), 32), :]
 
     pl.semaphore_wait(barrier, n_kv - 1 + n_tp - 1)
 
-    mine = pl.ds(pl.multiple_of(x * 64, 64), 64)
     sent_x = []
     for d in range(1, NX):
         to = (x + d) % NX
         peer = z * NX + to
-        sent_x.append(remote(tokp.at[x], tokp.at[x], xs.at[0, d], xr.at[0, d], peer, tp))
+        sent_x.append(remote(tokx.at[x], tokx.at[x], xs.at[0, d], xr.at[0, d], peer, tp))
         sent_x.append(remote(gp.at[x], gp.at[x], xs.at[1, d], xr.at[1, d], peer, tp))
         sent_x.append(
-            remote(wst.at[to], wcat.at[mine, pl.ds(0, 256)], xs.at[2, d], xr.at[2, d], peer, tp)
+            remote(wst.at[to], wcat.at[mine, :], xs.at[2, d], xr.at[2, d], peer, tp)
         )
     for copy in sent_x:
         copy.start()
@@ -279,7 +280,7 @@
         to = (z + d) % nz
         sent_t.append(
             remote(
-                tok_ref.at[pl.ds(pl.multiple_of(to * 32, 32), 32), :],
+                tokl.at[pl.ds(pl.multiple_of(to * 32, 32), 32), :],
                 tokt.at[z],
                 ts.at[d],
                 tr.at[d],
@@ -293,8 +294,7 @@
     def ring(way, step, what):
         to = (z + 1) % nz if way == 0 else (z + nz - 1) % nz
         block = (z + nz - (step - 1)) % nz if way == 0 else (z + step - 1) % nz
-        lanes = pl.ds(pl.multiple_of(block * 128, 128), 128)
-        ref = (out_all.at[:, lanes], up_all.at[block], down_all.at[:, lanes])[what]
+        ref = (out_all, up_all, down_all)[what].at[block]
         return remote(
             ref, ref, ring_s.at[way, step - 1, what], ring_r.at[way, step - 1, what], to * NX + x, tp
         )
@@ -321,9 +321,12 @@
 
     ring_start(1)
 
-    in_keys.wait()
-    in_vals.wait()
-    in_state.wait()
+    for copy in in_block:
+        copy.wait()
+    for i in range(4):
+        pairs = [(2 * i + j // 2, slice(j % 2, j % 2 + 1)) for j in range(4)]
+        bbeta[i] = jnp.concatenate([bbeta_ref[pair] for pair in pairs], axis=1)
+        bdecay[i] = jnp.concatenate([bdecay_ref[pair] for pair in pairs], axis=1)
 
     def before(g, carry):
         state_before(g, keys, vals, state, bbeta, bdecay, live_ref)
@@ -333,26 +336,19 @@
 
     for copy in sent_x:
         copy.wait_recv()
-    parts, squares = [], jnp.zeros((128, 128), F32)
-    for i in range(NX):
-        t = tokp[i].astype(F32)
-        squares = squares + t * t
-        parts.append(t * gp[i])
-    tops = jnp.concatenate([p[:, :64] for p in parts], axis=1)
-    bottoms = jnp.concatenate([p[:, 64:] for p in parts], axis=1)
-    normed = jnp.concatenate([tops, bottoms], axis=0).astype(BF16)
-    squares = jnp.concatenate(
-        [
-            jnp.sum(squares[:, :64], axis=1, keepdims=True),
-            jnp.sum(squares[:, 64:], axis=1, keepdims=True),
-        ],
-        axis=0,
-    )
+    t = tokx[...].reshape(256, 256).astype(F32).T
+    squares = jnp.sum(t * t, axis=1, keepdims=True)
+    normed = (t * jnp.concatenate([gp[i] for i in range(NX)], axis=1)).astype(BF16)
     projected = dot(normed, wcat[...])
-    proj_s[...] = projected[:, :256].reshape(n_kv, 8, 256).astype(BF16)
+    for copy in in_b:
+        copy.wait()
+    small = jnp.concatenate(
+        [bdw[...].astype(F32).reshape(32, 256), jnp.zeros((96, 256), F32)], axis=0
+    ).astype(BF16)
+    extra = dot_nt(normed, small)
+    proj_s[...] = projected.reshape(n_kv, 8, 256).astype(BF16)
     lane = iota((256, 128), 1)
     high = squares.astype(BF16).astype(F32)
-    extra = projected[:, 256:384]
     extra = jnp.where(lane == 32, high, jnp.where(lane == 33, squares - high, extra))
     ex_s[...] = extra.reshape(n_kv, 8, 128).astype(BF16)
     proj_r[kv] = proj_s[kv]
@@ -381,6 +377,8 @@
     all_extra.wait_recv()
     all_proj.wait_recv()
 
+    for copy in in_small:
+        copy.wait()
     total = jnp.sum(proj_r[...].astype(F32).reshape(nz, NX, 8, 256), axis=0)
     extra = jnp.sum(ex_r[...].astype(F32), axis=0)
     inverse_rms = lax.rsqrt((extra[:, 32:33] + extra[:, 33:34]) / MODEL + EPS)
@@ -446,9 +444,7 @@
         copy.wait_recv()
     ring_pass(4)
     m = mh[...].reshape(32, 256)
-    m = jnp.concatenate([m[:, :128], m[:, 128:]], axis=0).astype(BF16)
-    blocks = folded(dot(m, out_all[...]), nz)
-    ar[tp] = jnp.concatenate(blocks, axis=1).astype(BF16)
+    ar[tp] = dot_nt(m.astype(BF16), out_all[...].reshape(nz * 64, 256)).astype(BF16)
 
     def send_ar(d, carry):
         to = (tp + d) % n_tp
@@ -491,10 +487,9 @@
     rms = lax.rsqrt((total[:, 1024:1025] + total[:, 1025:1026]) / MODEL + EPS)
     hidden = jnp.maximum(total[:, :1024] * rms, 0.0)
     hidden = (hidden * hidden).astype(BF16)
-    hidden = jnp.concatenate([hidden[:, :512], hidden[:, 512:]], axis=0)
-    blocks = folded(dot(hidden, down_all[...]), nz)
+    output = dot_nt(hidden, down_all[...].reshape(nz * 64, 1024))
     for i in range(nz):
-        rs_s[i] = blocks[i].astype(BF16)
+        rs_s[i] = output[:, 64 * i : 64 * i + 64].astype(BF16)
     rs_r[tp] = rs_s[tp]
 
     def send_rs(d, carry):
@@ -547,8 +542,7 @@
         eight.wait_recv()
         eight.wait_send()
 
-    for i in range(nz):
-        mixed_ref[32 * i : 32 * i + 32, :] = mx[i]
+    mixed_ref[...] = mx[...].astype(F32).reshape(nz * 32, 64).T.astype(BF16)
 
 
 def body(
@@ -577,25 +571,30 @@
     n_tp = lax.axis_size("tp")
     nz = n_kv // NX
     vmem = pl.BlockSpec(memory_space=pltpu.VMEM)
-    smem = pl.BlockSpec(memory_space=pltpu.SMEM)
     hbm = pl.BlockSpec(memory_space=pl.ANY)
     dma = pltpu.SemaphoreType.DMA
-    return pl.pallas_call(
+    mixed, new_state = pl.pallas_call(
         functools.partial(kernel, n_kv=n_kv, n_tp=n_tp),
         out_shape=(
-            jax.ShapeDtypeStruct(tokens.shape, BF16),
+            jax.ShapeDtypeStruct(tokens.shape[::-1], BF16),
             jax.ShapeDtypeStruct(carried_state.shape, F32),
         ),
-        in_specs=[vmem, vmem, hbm, hbm, hbm, hbm, hbm, hbm, smem, vmem, hbm, hbm, hbm, vmem, vmem, smem, hbm, vmem, hbm, hbm],
+        in_specs=[hbm] * 20,
         out_specs=(vmem, hbm),
         scratch_shapes=[
             pltpu.VMEM((4, 64, 256), BF16),
-            pltpu.VMEM((256, 384), BF16),
-            pltpu.VMEM((256, 16), BF16),
-            pltpu.VMEM((256, 16), BF16),
-            pltpu.VMEM((NX, 128, 128), BF16),
-            pltpu.VMEM((NX, 1, 128), F32),
+            pltpu.VMEM((256, 256), BF16),
+            pltpu.VMEM((2, 16, 256), BF16),
+            pltpu.VMEM((NX, 64, 256), BF16),
+            pltpu.VMEM((NX, 1, 64), F32),
+            pltpu.VMEM((256, 64), BF16),
             pltpu.VMEM((nz, 32, 64), BF16),
+            pltpu.SMEM((2,), F32),
+            pltpu.VMEM((1, 128), F32),
+            pltpu.VMEM((8, 2, 64), F32),
+            pltpu.VMEM((8, 2, 64), F32),
+            pltpu.SMEM((8,), jnp.int32),
+            pltpu.VMEM((16, 128), F32),
             pltpu.VMEM((n_kv, 8, 256), BF16),
             pltpu.VMEM((n_kv, 8, 256), BF16),
             pltpu.VMEM((n_kv, 8, 128), BF16),
@@ -604,10 +603,8 @@
             pltpu.VMEM((8, 2, 64, 128), BF16),
             pltpu.VMEM((8, 2, 128, 128), F32),
             pltpu.VMEM((nz, 64, 1024), BF16),
-            pltpu.VMEM((512, 128 * nz), BF16),
-            pltpu.VMEM((128, 128 * nz), BF16),
-            pltpu.VMEM((1024, 64), BF16),
-            pltpu.VMEM((256, 64), BF16),
+            pltpu.VMEM((nz, 64, 1024), BF16),
+            pltpu.VMEM((nz, 64, 256), BF16),
             pltpu.VMEM((4, 1, 256), F32),
             pltpu.VMEM((4, 1, 256), F32),
             pltpu.VMEM((NX, 8, 256), F32),
@@ -618,7 +615,7 @@
             pltpu.VMEM((nz, 32, 64), F32),
             pltpu.VMEM((32, 64), BF16),
             pltpu.VMEM((nz, 32, 64), BF16),
-            dma((12,)),
+            dma((20,)),
             dma((3, NX)),
             dma((3, NX)),
             dma((nz,)),
@@ -639,18 +636,18 @@
             dma((2, 4, 3)),
         ],
         compiler_params=pltpu.CompilerParams(
-            collective_id=0, has_side_effects=True, vmem_limit_bytes=48 * 1024 * 1024
+            collective_id=0, has_side_effects=True
         ),
         name="layer",
     )(
-        tokens,
+        tokens.T,
         norm_gain.reshape(1, -1),
         query_weight,
         key_weight,
         value_weight,
         gate_weight,
-        beta_weight,
-        decay_weight,
+        beta_weight.T,
+        decay_weight.T,
         decay_rate,
         head_gain.reshape(1, -1),
         carried_state,
@@ -659,11 +656,12 @@
         block_beta,
         block_decay,
         live_count,
-        out_weight,
+        out_weight.T,
         mlp_gain.reshape(-1, 128),
         up_weight,
-        down_weight,
+        down_weight.T,
     )
+    return mixed.T, new_state
 
 
 def solution(mesh):

time: 83.7 us -> 69.8 us (0.83)
  local copies, waits for them, and re-layouts: 16.5 us -> 3.67 us
    unnamed x40 -> x2, local copies, waits for them, and re-layouts: 15 us -> 3.67 us
    pallas_call x1 -> x0, local copies, waits for them, and re-layouts: 1.54 us -> none  [body(): pl.pallas_call(functools.partial(kernel, n_kv=n_kv, n_tp=n_tp), out_shape...]
where the time goes in v2:
time: 69.8 us; the launch traced here: 69.6 us
  Pallas kernels  65.3 us (94%)
  local copies, waits for them, and re-layouts  3.67 us (5%)
    pallas_call x1, Pallas kernels, body(): pl.pallas_call(functools.partial(kernel, n_kv=n_kv, n_tp=n_tp), out_shape...  65.3 us
    unnamed x2, local copies, waits for them, and re-layouts  3.67 us

profile of v2, /device:TPU:1, one launch (start us, length us, event | category | flops | bytes accessed | tf_op | source)
XLA Modules:
  0.0 69.6 jit_solution(5781147842869533004)
XLA Ops:
  0.6 65.3 %layer.1 = (bf16[64,256]{1,0:T(8,128)(2,1)}, f32[8,2,128,128]{3,2,1,0:T(8,128)}) custom-call(bf16[64,256]{1,0:T(8,128)(2,1)} %bitcast.12, f32[1,64]{1,0:T(1,128)} %bitcast.16, bf16[64,256]{1,0:T(8,128)(2,1)} %qw_hbm.1, bf16[64,256]{1,0:T(8,128)(2,1)} %kw_hbm.1, bf16[64,256]{1,0:T(8,128)(2,1)} %vw_hbm.1, bf16[64,256]{1,0:T(8,128)(2,1)} %gw_hbm.1, ...), custom_call_target="tpu_custom_call" | custom-call | tf_op jit(solution)/shard_map/layer/pallas_call | solution.py:576
  65.9 1.4 %copy.24 = bf16[256,64]{0,1:T(8,128)(2,1)} copy(bf16[256,64]{0,1:T(8,128)(2,1)} %bitcast.14) | data formatting | bytes 65536
  67.3 2.3 %copy.25 = f32[8,2,128,128]{3,2,1,0:T(8,128)} copy(f32[8,2,128,128]{3,2,1,0:T(8,128)} %get-tuple-element.9) | data formatting | bytes 2097152

commit v3 on v2

--- a/solution.py
+++ b/solution.py
@@ -28,22 +28,35 @@
     return lax.dot_general(a, b, (((1,), (1,)), ((), ())), preferred_element_type=F32)
 
 
+def dot2(a, b):
+    bh, bl = split(b)
+    return dot(a, bh) + dot(a, bl)
+
+
+def iota(shape, dim):
+    return lax.broadcasted_iota(jnp.int32, shape, dim)
+
+
 def dot3(a, b):
     ah, al = split(a)
     bh, bl = split(b)
-    return dot(ah, bh) + (dot(ah, bl) + dot(al, bh))
-
-
-def dot2(a, b):
+    n = a.shape[0]
+    both = dot(jnp.concatenate([ah, al], axis=0), bh)
+    return both[:n] + both[n:] + dot(ah, bl)
+
+
+def apart(a, mask):
+    return jnp.concatenate([a] * 4, axis=0) * mask
+
+
+def dot3_blocks(a, b, mask):
+    ah, al = split(a)
     bh, bl = split(b)
-    return dot(a, bh) + dot(a, bl)
-
-
-def iota(shape, dim):
-    return lax.broadcasted_iota(jnp.int32, shape, dim)
-
-
-def unit_inverse(lower, r, c):
+    both = dot(jnp.concatenate([ah, al], axis=0), apart(bh, mask))
+    return both[:64] + both[64:] + dot(ah, apart(bl, mask))
+
+
+def unit_inverse(lower, r, c, mask):
     def same(bits):
         return (r >> bits) == (c >> bits)
 
@@ -51,54 +64,71 @@
     power = jnp.where(same(3), -lower, 0.0)
     total = ident + power
     for _ in range(2):
-        power = dot3(power, power)
-        total = total + dot3(total, power)
+        power = dot3_blocks(power, power, mask)
+        total = total + dot3_blocks(total, power, mask)
     for bits in (3, 4, 5):
         off = jnp.where(same(bits + 1) & jnp.logical_not(same(bits)), lower, 0.0)
-        total = total - dot3(total, dot3(off, total))
+        total = total - dot3_blocks(total, dot3_blocks(off, total, mask), mask)
     return total
 
 
-def state_before(g, keys, vals, state, bbeta, bdecay, live):
-    r = iota((256, 256), 0)
-    c = iota((256, 256), 1)
-    same = (r >> 6) == (c >> 6)
+def state_before(g, keys, vals, state, bbeta, bdecay, live, mask_ref):
+    mask = mask_ref[...]
+    r = iota((64, 256), 0)
+    lane = iota((64, 256), 1)
+    c = lane & 63
+    pair = lane >> 6
     n0, n1 = live[2 * g] - 1, live[2 * g + 1] - 1
-    lane = iota((1, 256), 1)
-    live_row = (lane & 63) < jnp.where(lane < 128, n0, n1)
+    lane1 = iota((1, 256), 1)
+    live_row = (lane1 & 63) < jnp.where(lane1 < 128, n0, n1)
     d_row = jnp.where(live_row, bdecay[g], 0.0)
     b_row = jnp.where(live_row, bbeta[g], 0.0)
     r1 = iota((256, 128), 0)
     live_col = (r1 & 63) < jnp.where(r1 < 128, n0, n1)
     k_all = jnp.where(live_col, keys[pl.ds(2 * g, 2)].astype(F32).reshape(256, 128), 0.0)
     v_all = jnp.where(live_col, vals[pl.ds(2 * g, 2)].astype(F32).reshape(256, 128), 0.0)
-    d_col = jnp.sum(jnp.where(r == c, d_row, 0.0), axis=1, keepdims=True)
-    b_col = jnp.sum(jnp.where(r == c, b_row, 0.0), axis=1, keepdims=True)
-    tot_col = jnp.sum(jnp.where(same & (c <= r), d_row, 0.0), axis=1, keepdims=True)
-    tot_row = jnp.sum(jnp.where(same & (r <= c), d_col, 0.0), axis=0, keepdims=True)
-    end_col = jnp.sum(jnp.where(same, d_row, 0.0), axis=1, keepdims=True)
     kb = k_all.astype(BF16)
     kt = k_all.T.astype(BF16)
-    strict = same & (c < r)
-    fade = jnp.exp(jnp.where(strict, tot_col - tot_row, 0.0))
-    lower = jnp.where(strict, b_col * dot(kb, kt) * fade, 0.0)
-    inverse = unit_inverse(lower, r, c)
-    old = jnp.concatenate([state[2 * g + p // 2, p % 2] for p in range(4)], axis=1)
-    seen = dot2(kb, old)
-    seen = jnp.concatenate(
-        [seen[64 * p : 64 * p + 64, 128 * p : 128 * p + 128] for p in range(4)], axis=0
-    )
-    right = b_col * (v_all - jnp.exp(tot_col) * seen)
-    update = dot3(inverse, right) * jnp.exp(end_col - tot_col)
-    r4 = iota((256, 512), 0)
-    c4 = iota((256, 512), 1)
-    wide = jnp.concatenate([update] * 4, axis=1)
-    wide = jnp.where((r4 >> 6) == (c4 >> 7), wide, 0.0)
-    added = dot2(kt, wide)
+    b_diag = jnp.where(r == c, b_row, 0.0)
+    d_tri = jnp.where(c <= r, d_row, 0.0)
+    b_col, t_col = [], []
     for p in range(4):
-        end = jnp.exp(end_col[64 * p : 64 * p + 1, :])
-        at = slice(128 * p, 128 * p + 128)
-        state[2 * g + p // 2, p % 2] = end * old[:, at] + added[:, at]
+        b_col.append(jnp.sum(jnp.where(pair == p, b_diag, 0.0), axis=1, keepdims=True))
+        t_col.append(jnp.sum(jnp.where(pair == p, d_tri, 0.0), axis=1, keepdims=True))
+
+    def side(columns):
+        low = jnp.where(pair == 0, columns[0], columns[1])
+        high = jnp.where(pair == 2, columns[2], columns[3])
+        return jnp.where(pair < 2, low, high)
+
+    tots = side(t_col)
+    tot_row = jnp.sum(jnp.where(r == c, tots, 0.0), axis=0, keepdims=True)
+    strict = c < r
+    fade = jnp.exp(jnp.where(strict, tots - tot_row, 0.0))
+    gram = dot(kb, kt)
+    gram = side([gram[64 * p : 64 * p + 64] for p in range(4)])
+    lower = jnp.where(strict, side(b_col) * gram * fade, 0.0)
+    inverse = unit_inverse(lower, r, c, mask)
+    zero = jnp.zeros((64, 128), F32)
+
+    def spread(blocks):
+        rows = [[blocks[p] if q == p else zero for q in range(4)] for p in range(4)]
+        return jnp.concatenate([jnp.concatenate(row, axis=1) for row in rows], axis=0)
+
+    right = []
+    for p in range(4):
+        at = slice(64 * p, 64 * p + 64)
+        seen = dot2(kb[at], state[2 * g + p // 2, p % 2])
+        right.append(b_col[p] * (v_all[at] - jnp.exp(t_col[p]) * seen))
+    update = dot3(inverse, spread(right))
+    faded = []
+    for p in range(4):
+        faded.append(update[:, 128 * p : 128 * p + 128] * jnp.exp(t_col[p][63:64] - t_col[p]))
+    added = dot2(kt, spread(faded))
+    for p in range(4):
+        end = jnp.exp(t_col[p][63:64])
+        at = (2 * g + p // 2, p % 2)
+        state[at] = end * state[at] + added[:, 128 * p : 128 * p + 128]
 
 
 def kernel(
@@ -123,7 +153,7 @@
     up_hbm,
     down_hbm,
     mixed_ref,
-    nstate_hbm,
+    state,
     wst,
     wcat,
     bdw,
@@ -143,7 +173,7 @@
     ex_r,
     keys,
     vals,
-    state,
+    mask,
     up_all,
     down_all,
     out_all,
@@ -176,6 +206,7 @@
     fr,
     ring_s,
     ring_r,
+    round_r,
     *,
     n_kv,
     n_tp,
@@ -226,29 +257,39 @@
         local(mgain_hbm, mgain_ref, 19),
     ]
 
+    up_z = ((z + 1) % nz) * NX + x
+    down_z = ((z + nz - 1) % nz) * NX + x
     barrier = pltpu.get_barrier_semaphore()
 
-    def greet_kv(d, carry):
+    def greet(sem, kv_to, tp_to):
         pl.semaphore_signal(
-            barrier,
+            sem,
             inc=1,
-            device_id={"kv": (kv + d) % n_kv, "tp": tp},
+            device_id={"kv": kv_to, "tp": tp_to},
             device_id_type=pl.DeviceIdType.MESH,
         )
+
+    greet(barrier, up_z, tp)
+    greet(barrier, down_z, tp)
+    for d in range(1, NX):
+        greet(barrier, z * NX + (x + d) % NX, tp)
+
+    def greet_tp(d, carry):
+        greet(barrier, kv, (tp + d) % n_tp)
         return carry
 
-    def greet_tp(d, carry):
-        pl.semaphore_signal(
-            barrier,
-            inc=1,
-            device_id={"kv": kv, "tp": (tp + d) % n_tp},
-            device_id_type=pl.DeviceIdType.MESH,
-        )
-        return carry
-
-    lax.fori_loop(1, n_kv, greet_kv, 0)
     lax.fori_loop(1, n_tp, greet_tp, 0)
 
+    def round_send(i):
+        greet(round_r.at[i], up_z, tp)
+        greet(round_r.at[i], down_z, tp)
+
+    def round_wait(i):
+        pl.semaphore_wait(round_r.at[i], 2)
+
+    mask[...] = jnp.where((iota((256, 256), 0) >> 6) == (iota((256, 256), 1) >> 6), 1.0, 0.0).astype(
+        BF16
+    )
     in_tok.wait()
     in_gain.wait()
     tokl[...] = tokx[x].astype(F32).T.astype(BF16)
@@ -261,7 +302,7 @@
     in_up.wait()
     in_down.wait()
 
-    pl.semaphore_wait(barrier, n_kv - 1 + n_tp - 1)
+    pl.semaphore_wait(barrier, 2 + NX - 1 + n_tp - 1)
 
     sent_x = []
     for d in range(1, NX):
@@ -288,15 +329,12 @@
                 tp,
             )
         )
-    for copy in sent_t:
-        copy.start()
-
     def ring(way, step, what):
-        to = (z + 1) % nz if way == 0 else (z + nz - 1) % nz
+        to = up_z if way == 0 else down_z
         block = (z + nz - (step - 1)) % nz if way == 0 else (z + step - 1) % nz
         ref = (out_all, up_all, down_all)[what].at[block]
         return remote(
-            ref, ref, ring_s.at[way, step - 1, what], ring_r.at[way, step - 1, what], to * NX + x, tp
+            ref, ref, ring_s.at[way, step - 1, what], ring_r.at[way, step - 1, what], to, tp
         )
 
     half = nz // 2
@@ -309,17 +347,24 @@
             if step < half or way == (1 if what == 2 else 0)
         ]
 
-    def ring_start(step):
-        for way, what in plan[step]:
+    OUT, UP, DOWN = 0, 1, 2
+
+    def ways(step, what):
+        return [way for way in range(2) if (way, what) in plan.get(step, ())]
+
+    def ring_start(step, what):
+        for way in ways(step, what):
             ring(way, step, what).start()
 
-    def ring_pass(step):
-        for way, what in plan[step]:
+    def ring_pass(step, what):
+        for way in ways(step, what):
             ring(way, step, what).wait_recv()
-            if step < half and (way, what) in plan[step + 1]:
+            if way in ways(step + 1, what):
                 ring(way, step + 1, what).start()
 
-    ring_start(1)
+    ring_start(1, OUT)
+    ring_start(1, UP)
+    round_send(0)
 
     for copy in in_block:
         copy.wait()
@@ -329,13 +374,22 @@
         bdecay[i] = jnp.concatenate([bdecay_ref[pair] for pair in pairs], axis=1)
 
     def before(g, carry):
-        state_before(g, keys, vals, state, bbeta, bdecay, live_ref)
+        state_before(g, keys, vals, state, bbeta, bdecay, live_ref, mask)
         return carry
 
-    lax.fori_loop(0, 2, before, 0)
+    lax.fori_loop(0, 1, before, 0)
+    round_wait(0)
+    round_send(1)
+    ring_pass(1, OUT)
+    ring_start(1, DOWN)
+    lax.fori_loop(1, 2, before, 0)
+    round_wait(1)
+    round_send(2)
 
     for copy in sent_x:
         copy.wait_recv()
+    round_wait(2)
+    round_send(3)
     t = tokx[...].reshape(256, 256).astype(F32).T
     squares = jnp.sum(t * t, axis=1, keepdims=True)
     normed = (t * jnp.concatenate([gp[i] for i in range(NX)], axis=1)).astype(BF16)
@@ -364,11 +418,19 @@
         remote(ex_s.at[to], ex_r.at[z], ps.at[1], pr.at[1], to, tp).start()
         return carry
 
+    round_wait(3)
     lax.fori_loop(1, nz, send_extra, 0)
     lax.fori_loop(1, n_kv, send_proj, 0)
-
-    ring_pass(1)
-    lax.fori_loop(2, 4, before, 0)
+    for copy in sent_t:
+        copy.start()
+
+    ring_pass(1, UP)
+    ring_pass(2, OUT)
+    lax.fori_loop(2, 3, before, 0)
+    ring_pass(1, DOWN)
+    lax.fori_loop(3, 4, before, 0)
+    ring_pass(2, UP)
+    ring_pass(3, OUT)
 
     some = pl.ds(0, n_kv - 1)
     few = pl.ds(0, nz - 1)
@@ -430,19 +492,18 @@
         sent_m.append(remote(mh.at[x], mh.at[x], ms.at[d], mr.at[d], peer, tp))
     for copy in sent_m:
         copy.start()
-    ring_pass(2)
+    ring_pass(2, DOWN)
 
     for h in range(2):
         e = heads[h][4]
         for s in range(8):
             kcol = columns[:, 16 * h + s : 16 * h + s + 1]
             state[s, h] = e[s : s + 1] * state[s, h] + kcol * updates[s, h]
-    put_state = local(state, nstate_hbm, 0)
-    ring_pass(3)
+    ring_pass(3, UP)
 
     for copy in sent_m:
         copy.wait_recv()
-    ring_pass(4)
+    ring_pass(4, OUT)
     m = mh[...].reshape(32, 256)
     ar[tp] = dot_nt(m.astype(BF16), out_all[...].reshape(nz * 64, 256)).astype(BF16)
 
@@ -452,6 +513,7 @@
         return carry
 
     lax.fori_loop(1, n_tp, send_ar, 0)
+    ring_pass(3, DOWN)
     tps = pl.ds(0, n_tp - 1)
     all_ar = remote(ar.at[tps], ar.at[tps], asem, arr, kv, tp)
     for copy in sent_t:
@@ -470,6 +532,7 @@
         resid[i] = residual[:, 64 * i : 64 * i + 64]
     squares = jnp.sum(residual * residual, axis=1, keepdims=True)
     mlp_in = (residual * gains).astype(BF16)
+    ring_pass(4, UP)
     pre = dot(mlp_in, up_all[...].reshape(nz * 64, 1024))
     high = squares.astype(BF16).astype(F32)
     lane = iota((32, 128), 1)
@@ -481,6 +544,7 @@
         sent_u.append(remote(ax.at[x], ax.at[x], us.at[d], ur.at[d], peer, tp))
     for copy in sent_u:
         copy.start()
+    ring_pass(4, DOWN)
     for copy in sent_u:
         copy.wait_recv()
     total = jnp.sum(ax[...].astype(F32), axis=0)
@@ -518,7 +582,6 @@
 
     lax.fori_loop(0, n_tp, send_fin, 0)
 
-    put_state.wait()
     for copy in sent_x + sent_t + sent_m + sent_u:
         copy.wait_send()
     for step in plan:
@@ -571,8 +634,30 @@
     n_tp = lax.axis_size("tp")
     nz = n_kv // NX
     vmem = pl.BlockSpec(memory_space=pltpu.VMEM)
-    hbm = pl.BlockSpec(memory_space=pl.ANY)
+    hbm = pl.BlockSpec(memory_space=pltpu.HBM)
     dma = pltpu.SemaphoreType.DMA
+    operands = (
+        tokens.T,
+        norm_gain.reshape(1, -1),
+        query_weight,
+        key_weight,
+        value_weight,
+        gate_weight,
+        beta_weight.T,
+        decay_weight.T,
+        decay_rate,
+        head_gain.reshape(1, -1),
+        carried_state,
+        block_keys,
+        block_values,
+        block_beta,
+        block_decay,
+        live_count,
+        out_weight.T,
+        mlp_gain.reshape(-1, 128),
+        up_weight,
+        down_weight.T,
+    )
     mixed, new_state = pl.pallas_call(
         functools.partial(kernel, n_kv=n_kv, n_tp=n_tp),
         out_shape=(
@@ -580,7 +665,7 @@
             jax.ShapeDtypeStruct(carried_state.shape, F32),
         ),
         in_specs=[hbm] * 20,
-        out_specs=(vmem, hbm),
+        out_specs=(vmem, vmem),
         scratch_shapes=[
             pltpu.VMEM((4, 64, 256), BF16),
             pltpu.VMEM((256, 256), BF16),
@@ -601,7 +686,7 @@
             pltpu.VMEM((nz, 8, 128), BF16),
             pltpu.VMEM((8, 2, 64, 128), BF16),
             pltpu.VMEM((8, 2, 64, 128), BF16),
-            pltpu.VMEM((8, 2, 128, 128), F32),
+            pltpu.VMEM((256, 256), BF16),
             pltpu.VMEM((nz, 64, 1024), BF16),
             pltpu.VMEM((nz, 64, 1024), BF16),
             pltpu.VMEM((nz, 64, 256), BF16),
@@ -634,33 +719,13 @@
             dma,
             dma((2, 4, 3)),
             dma((2, 4, 3)),
+            pltpu.SemaphoreType.REGULAR((4,)),
         ],
         compiler_params=pltpu.CompilerParams(
-            collective_id=0, has_side_effects=True
+            collective_id=0, has_side_effects=True, vmem_limit_bytes=40 * 1024 * 1024
         ),
         name="layer",
-    )(
-        tokens.T,
-        norm_gain.reshape(1, -1),
-        query_weight,
-        key_weight,
-        value_weight,
-        gate_weight,
-        beta_weight.T,
-        decay_weight.T,
-        decay_rate,
-        head_gain.reshape(1, -1),
-        carried_state,
-        block_keys,
-        block_values,
-        block_beta,
-        block_decay,
-        live_count,
-        out_weight.T,
-        mlp_gain.reshape(-1, 128),
-        up_weight,
-        down_weight.T,
-    )
+    )(*[pltpu.with_memory_space_constraint(a, pltpu.HBM) for a in operands])
     return mixed.T, new_state
 
 

time: 69.8 us -> 60 us (0.86)
  Pallas kernels: 65.3 us -> 57.7 us
  local copies, waits for them, and re-layouts: 3.67 us -> 1.59 us
    pallas_call x1, Pallas kernels: 65.3 us -> 57.7 us  [body(): pl.pallas_call(functools.partial(kernel, n_kv=n_kv, n_tp=n_tp), out_shape...]
    unnamed x2, local copies, waits for them, and re-layouts: 3.67 us -> 1.59 us
where the time goes in v3:
time: 60 us; the launch traced here: 59.9 us
  Pallas kernels  57.7 us (96%)
  local copies, waits for them, and re-layouts  1.59 us (3%)
  between operations  0.65 us (1%)
    pallas_call x1, Pallas kernels, body(): pl.pallas_call(functools.partial(kernel, n_kv=n_kv, n_tp=n_tp), out_shape...  57.7 us
    unnamed x2, local copies, waits for them, and re-layouts  1.59 us

profile of v3, /device:TPU:1, one launch (start us, length us, event | category | flops | bytes accessed | tf_op | source)
XLA Modules:
  0.0 59.9 jit_solution(5118855024994597889)
XLA Ops:
  0.6 57.7 %layer.1 = (bf16[64,256]{1,0:T(8,128)(2,1)S(1)}, f32[8,2,128,128]{3,2,1,0:T(8,128)S(1)}) custom-call(bf16[64,256]{1,0:T(8,128)(2,1)} %bitcast.13, f32[1,64]{1,0:T(1,128)} %bitcast.16, bf16[64,256]{1,0:T(8,128)(2,1)} %qw_hbm.1, bf16[64,256]{1,0:T(8,128)(2,1)} %kw_hbm.1, bf16[64,256]{1,0:T(8,128)(2,1)} %vw_hbm.1, bf16[64,256]{1,0:T(8,128)(2,1)} %gw_hbm.1, ...), custom_call_target="tpu_custom_call" | custom-call | tf_op jit(solution)/shard_map/layer/pallas_call | solution.py:661
  58.3 0.6 %copy.24 = bf16[256,64]{0,1:T(8,128)(2,1)} copy(bf16[256,64]{0,1:T(8,128)(2,1)S(1)} %bitcast.9) | data formatting | bytes 65536
  59.0 1.0 %copy.25 = f32[8,2,128,128]{3,2,1,0:T(8,128)} copy(f32[8,2,128,128]{3,2,1,0:T(8,128)S(1)} %get-tuple-element.9) | data formatting | bytes 2097152

commit v4 on v3

--- a/solution.py
+++ b/solution.py
@@ -182,8 +182,7 @@
     mh,
     ar,
     ax,
-    rs_s,
-    rs_r,
+    rs,
     resid,
     fin_s,
     mx,
@@ -269,8 +268,9 @@
             device_id_type=pl.DeviceIdType.MESH,
         )
 
-    greet(barrier, up_z, tp)
-    greet(barrier, down_z, tp)
+    near_z = [((z + d) % nz) * NX + x for d in (1, nz - 1, 2, nz - 2)]
+    for to in near_z:
+        greet(barrier, to, tp)
     for d in range(1, NX):
         greet(barrier, z * NX + (x + d) % NX, tp)
 
@@ -281,11 +281,11 @@
     lax.fori_loop(1, n_tp, greet_tp, 0)
 
     def round_send(i):
-        greet(round_r.at[i], up_z, tp)
-        greet(round_r.at[i], down_z, tp)
+        for to in near_z:
+            greet(round_r.at[i], to, tp)
 
     def round_wait(i):
-        pl.semaphore_wait(round_r.at[i], 2)
+        pl.semaphore_wait(round_r.at[i], 4)
 
     mask[...] = jnp.where((iota((256, 256), 0) >> 6) == (iota((256, 256), 1) >> 6), 1.0, 0.0).astype(
         BF16
@@ -302,7 +302,7 @@
     in_up.wait()
     in_down.wait()
 
-    pl.semaphore_wait(barrier, 2 + NX - 1 + n_tp - 1)
+    pl.semaphore_wait(barrier, 4 + NX - 1 + n_tp - 1)
 
     sent_x = []
     for d in range(1, NX):
@@ -332,39 +332,33 @@
     def ring(way, step, what):
         to = up_z if way == 0 else down_z
         block = (z + nz - (step - 1)) % nz if way == 0 else (z + step - 1) % nz
-        ref = (out_all, up_all, down_all)[what].at[block]
+        ref = (out_all, up_all, down_all, down_all)[what].at[block]
+        first, rows = (0, 64) if what < 2 else (32 * (what - 2), 32)
+        if step == nz // 2:
+            first, rows = first + rows // 2 * way, rows // 2
+        ref = ref.at[pl.ds(first, rows)]
         return remote(
             ref, ref, ring_s.at[way, step - 1, what], ring_r.at[way, step - 1, what], to, tp
         )
 
     half = nz // 2
-    plan = {}
-    for step in range(1, half + 1):
-        plan[step] = [
-            (way, what)
-            for what in range(3)
-            for way in range(2)
-            if step < half or way == (1 if what == 2 else 0)
-        ]
-
-    OUT, UP, DOWN = 0, 1, 2
-
-    def ways(step, what):
-        return [way for way in range(2) if (way, what) in plan.get(step, ())]
 
     def ring_start(step, what):
-        for way in ways(step, what):
+        for way in range(2):
             ring(way, step, what).start()
 
     def ring_pass(step, what):
-        for way in ways(step, what):
+        for way in range(2):
             ring(way, step, what).wait_recv()
-            if way in ways(step + 1, what):
+            if step < half:
                 ring(way, step + 1, what).start()
 
+    OUT, UP, LOW, HIGH = 0, 1, 2, 3
+
+    round_send(0)
     ring_start(1, OUT)
     ring_start(1, UP)
-    round_send(0)
+    ring_start(1, LOW)
 
     for copy in in_block:
         copy.wait()
@@ -381,15 +375,10 @@
     round_wait(0)
     round_send(1)
     ring_pass(1, OUT)
-    ring_start(1, DOWN)
     lax.fori_loop(1, 2, before, 0)
-    round_wait(1)
-    round_send(2)
 
     for copy in sent_x:
         copy.wait_recv()
-    round_wait(2)
-    round_send(3)
     t = tokx[...].reshape(256, 256).astype(F32).T
     squares = jnp.sum(t * t, axis=1, keepdims=True)
     normed = (t * jnp.concatenate([gp[i] for i in range(NX)], axis=1)).astype(BF16)
@@ -409,7 +398,9 @@
     ex_r[z] = ex_s[kv]
 
     def send_proj(d, carry):
-        to = (kv + d) % n_kv
+        far = d // NX
+        far = nz // 2 + (far + 1) // 2 * (1 - 2 * (far % 2))
+        to = ((z + far) % nz) * NX + (x + NX - 1 - d % NX) % NX
         remote(proj_s.at[to], proj_r.at[kv], ps.at[0], pr.at[0], to, tp).start()
         return carry
 
@@ -418,19 +409,19 @@
         remote(ex_s.at[to], ex_r.at[z], ps.at[1], pr.at[1], to, tp).start()
         return carry
 
-    round_wait(3)
+    round_wait(1)
     lax.fori_loop(1, nz, send_extra, 0)
-    lax.fori_loop(1, n_kv, send_proj, 0)
+    lax.fori_loop(0, n_kv - 1, send_proj, 0)
+    ring_pass(1, UP)
+    lax.fori_loop(2, 3, before, 0)
+    ring_pass(2, OUT)
+    ring_pass(1, LOW)
+    ring_start(1, HIGH)
+    lax.fori_loop(3, 4, before, 0)
+    ring_pass(3, OUT)
+    ring_pass(2, UP)
     for copy in sent_t:
         copy.start()
-
-    ring_pass(1, UP)
-    ring_pass(2, OUT)
-    lax.fori_loop(2, 3, before, 0)
-    ring_pass(1, DOWN)
-    lax.fori_loop(3, 4, before, 0)
-    ring_pass(2, UP)
-    ring_pass(3, OUT)
 
     some = pl.ds(0, n_kv - 1)
     few = pl.ds(0, nz - 1)
@@ -492,14 +483,14 @@
         sent_m.append(remote(mh.at[x], mh.at[x], ms.at[d], mr.at[d], peer, tp))
     for copy in sent_m:
         copy.start()
-    ring_pass(2, DOWN)
-
+    ring_pass(2, LOW)
     for h in range(2):
         e = heads[h][4]
         for s in range(8):
             kcol = columns[:, 16 * h + s : 16 * h + s + 1]
             state[s, h] = e[s : s + 1] * state[s, h] + kcol * updates[s, h]
-    ring_pass(3, UP)
+
+    ring_pass(1, HIGH)
 
     for copy in sent_m:
         copy.wait_recv()
@@ -513,7 +504,7 @@
         return carry
 
     lax.fori_loop(1, n_tp, send_ar, 0)
-    ring_pass(3, DOWN)
+    ring_pass(3, UP)
     tps = pl.ds(0, n_tp - 1)
     all_ar = remote(ar.at[tps], ar.at[tps], asem, arr, kv, tp)
     for copy in sent_t:
@@ -524,12 +515,13 @@
         gain = mgain_ref[pl.ds(2 * p + x // 2, 1), :]
         gains.append(jnp.where(x % 2 == 0, gain[:, :64], gain[:, 64:]))
     gains = jnp.concatenate(gains, axis=1)
+    ring_pass(3, LOW)
     all_ar.wait_recv()
+    ring_pass(2, HIGH)
 
     attended = jnp.sum(ar[...].astype(F32), axis=0)
     residual = (tokens + attended).astype(BF16).astype(F32)
-    for i in range(nz):
-        resid[i] = residual[:, 64 * i : 64 * i + 64]
+    resid[...] = residual
     squares = jnp.sum(residual * residual, axis=1, keepdims=True)
     mlp_in = (residual * gains).astype(BF16)
     ring_pass(4, UP)
@@ -544,68 +536,63 @@
         sent_u.append(remote(ax.at[x], ax.at[x], us.at[d], ur.at[d], peer, tp))
     for copy in sent_u:
         copy.start()
-    ring_pass(4, DOWN)
+    ring_pass(3, HIGH)
     for copy in sent_u:
         copy.wait_recv()
+    ring_pass(4, LOW)
+    ring_pass(4, HIGH)
     total = jnp.sum(ax[...].astype(F32), axis=0)
     rms = lax.rsqrt((total[:, 1024:1025] + total[:, 1025:1026]) / MODEL + EPS)
     hidden = jnp.maximum(total[:, :1024] * rms, 0.0)
     hidden = (hidden * hidden).astype(BF16)
     output = dot_nt(hidden, down_all[...].reshape(nz * 64, 1024))
-    for i in range(nz):
-        rs_s[i] = output[:, 64 * i : 64 * i + 64].astype(BF16)
-    rs_r[tp] = rs_s[tp]
+    rs[tp] = output.astype(BF16)
 
     def send_rs(d, carry):
         to = (tp + d) % n_tp
-        remote(rs_s.at[to], rs_r.at[tp], ds_, dr, kv, to).start()
+        remote(rs.at[tp], rs.at[tp], ds_, dr, kv, to).start()
         return carry
 
     lax.fori_loop(1, n_tp, send_rs, 0)
-    all_rs = remote(rs_s.at[tps], rs_r.at[tps], ds_, dr, kv, tp)
+    all_rs = remote(rs.at[tps], rs.at[tps], ds_, dr, kv, tp)
     all_rs.wait_recv()
-    fin_s[...] = (resid[tp] + jnp.sum(rs_r[...].astype(F32), axis=0)).astype(BF16)
-
-    at_home = z == tp
-    far = tp * NX + x
-
-    def send_fin(t, carry):
-        @pl.when(jnp.logical_or(jnp.logical_not(at_home), t != tp))
-        def _():
-            remote(fin_s, mx.at[z], fs, fr, far, t).start()
-
-        return carry
-
-    @pl.when(at_home)
-    def _():
-        mx[z] = fin_s[...]
-
-    lax.fori_loop(0, n_tp, send_fin, 0)
-
-    for copy in sent_x + sent_t + sent_m + sent_u:
+    final = resid[...] + jnp.sum(rs[...].astype(F32), axis=0)
+    for i in range(nz):
+        fin_s[i] = final[:, 64 * i : 64 * i + 64].astype(BF16)
+    mx[z] = fin_s[z]
+
+    sent_f = []
+    for d in range(1, nz):
+        to = (z + d) % nz
+        sent_f.append(remote(fin_s.at[to], mx.at[z], fs.at[d], fr.at[d], to * NX + x, tp))
+    for copy in sent_f:
+        copy.start()
+
+    for copy in sent_x + sent_t + sent_m + sent_u + sent_f:
         copy.wait_send()
-    for step in plan:
-        for way, what in plan[step]:
-            ring(way, step, what).wait_send()
+    for step in range(1, half + 1):
+        for way in range(2):
+            for what in (OUT, UP, LOW, HIGH):
+                ring(way, step, what).wait_send()
     all_proj.wait_send()
     all_extra.wait_send()
     all_ar.wait_send()
     all_rs.wait_send()
 
-    eight = remote(mx, mx, fs, fr, kv, tp)
-    seven = remote(mx.at[few], mx.at[few], fs, fr, kv, tp)
-
-    @pl.when(at_home)
-    def _():
-        seven.wait_recv()
-        seven.wait_send()
-
-    @pl.when(jnp.logical_not(at_home))
-    def _():
-        eight.wait_recv()
-        eight.wait_send()
-
+    for copy in sent_f:
+        copy.wait_recv()
     mixed_ref[...] = mx[...].astype(F32).reshape(nz * 32, 64).T.astype(BF16)
+
+
+def put(mixed, state, mixed_hbm, state_hbm, sem):
+    copies = [
+        pltpu.make_async_copy(state, state_hbm, sem.at[0]),
+        pltpu.make_async_copy(mixed, mixed_hbm, sem.at[1]),
+    ]
+    for copy in copies:
+        copy.start()
+    for copy in copies:
+        copy.wait()
 
 
 def body(
@@ -695,10 +682,9 @@
             pltpu.VMEM((NX, 8, 256), F32),
             pltpu.VMEM((n_tp, 32, 512), BF16),
             pltpu.VMEM((NX, 32, 1152), BF16),
-            pltpu.VMEM((n_tp, 32, 64), BF16),
-            pltpu.VMEM((n_tp, 32, 64), BF16),
-            pltpu.VMEM((nz, 32, 64), F32),
-            pltpu.VMEM((32, 64), BF16),
+            pltpu.VMEM((n_tp, 32, 512), BF16),
+            pltpu.VMEM((32, 512), F32),
+            pltpu.VMEM((nz, 32, 64), BF16),
             pltpu.VMEM((nz, 32, 64), BF16),
             dma((20,)),
             dma((3, NX)),
@@ -715,17 +701,29 @@
             dma((NX,)),
             dma,
             dma,
-            dma,
-            dma,
-            dma((2, 4, 3)),
-            dma((2, 4, 3)),
-            pltpu.SemaphoreType.REGULAR((4,)),
+            dma((nz,)),
+            dma((nz,)),
+            dma((2, 4, 4)),
+            dma((2, 4, 4)),
+            pltpu.SemaphoreType.REGULAR((2,)),
         ],
         compiler_params=pltpu.CompilerParams(
             collective_id=0, has_side_effects=True, vmem_limit_bytes=40 * 1024 * 1024
         ),
         name="layer",
     )(*[pltpu.with_memory_space_constraint(a, pltpu.HBM) for a in operands])
+    mixed, new_state = pl.pallas_call(
+        put,
+        out_shape=(
+            jax.ShapeDtypeStruct(mixed.shape, BF16),
+            jax.ShapeDtypeStruct(new_state.shape, F32),
+        ),
+        in_specs=[vmem, vmem],
+        out_specs=(hbm, hbm),
+        scratch_shapes=[dma((2,))],
+        compiler_params=pltpu.CompilerParams(vmem_limit_bytes=16 * 1024 * 1024),
+        name="put",
+    )(mixed, new_state)
     return mixed.T, new_state
 
 

time: 60 us -> 54.4 us (0.907)
  Pallas kernels: 57.7 us -> 53.7 us
  local copies, waits for them, and re-layouts: 1.59 us -> 0 us
    pallas_call x1, Pallas kernels: 57.7 us -> 52.7 us  [body(): pl.pallas_call(functools.partial(kernel, n_kv=n_kv, n_tp=n_tp), out_shape...]
    unnamed x2 -> x0, local copies, waits for them, and re-layouts: 1.59 us -> none
    pallas_call x0 -> x1, Pallas kernels: none -> 0.99 us  [body(): pl.pallas_call(put, out_shape=(jax.ShapeDtypeStruct(mixed.shape, BF16), j...]
where the time goes in v4:
time: 54.4 us; the launch traced here: 54.3 us
  Pallas kernels  53.7 us (99%)
  between operations  0.65 us (1%)
    pallas_call x1, Pallas kernels, body(): pl.pallas_call(functools.partial(kernel, n_kv=n_kv, n_tp=n_tp), out_shape...  52.7 us

profile of v4, /device:TPU:1, one launch (start us, length us, event | category | flops | bytes accessed | tf_op | source)
XLA Modules:
  0.0 54.3 jit_solution(13386563805312723605)
XLA Ops:
  0.6 52.7 %layer.1 = (bf16[64,256]{1,0:T(8,128)(2,1)S(1)}, f32[8,2,128,128]{3,2,1,0:T(8,128)S(1)}) custom-call(bf16[64,256]{1,0:T(8,128)(2,1)} %bitcast.12, f32[1,64]{1,0:T(1,128)} %bitcast.15, bf16[64,256]{1,0:T(8,128)(2,1)} %qw_hbm.1, bf16[64,256]{1,0:T(8,128)(2,1)} %kw_hbm.1, bf16[64,256]{1,0:T(8,128)(2,1)} %vw_hbm.1, bf16[64,256]{1,0:T(8,128)(2,1)} %gw_hbm.1, ...), custom_call_target="tpu_custom_call" | custom-call | tf_op jit(solution)/shard_map/layer/pallas_call | solution.py:648
  53.3 1.0 %put.1 = (bf16[64,256]{1,0:T(8,128)(2,1)}, f32[8,2,128,128]{3,2,1,0:T(8,128)}) custom-call(bf16[64,256]{1,0:T(8,128)(2,1)S(1)} %get-tuple-element.6.mixed, f32[8,2,128,128]{3,2,1,0:T(8,128)S(1)} %get-tuple-element.7.state), custom_call_target="tpu_custom_call" | custom-call | tf_op jit(solution)/shard_map/put/pallas_call | solution.py:715

commit v5 on v4

--- a/solution.py
+++ b/solution.py
@@ -56,79 +56,89 @@
     return both[:64] + both[64:] + dot(ah, apart(bl, mask))
 
 
-def unit_inverse(lower, r, c, mask):
-    def same(bits):
-        return (r >> bits) == (c >> bits)
-
-    ident = jnp.where(r == c, 1.0, 0.0)
-    power = jnp.where(same(3), -lower, 0.0)
-    total = ident + power
-    for _ in range(2):
-        power = dot3_blocks(power, power, mask)
-        total = total + dot3_blocks(total, power, mask)
-    for bits in (3, 4, 5):
-        off = jnp.where(same(bits + 1) & jnp.logical_not(same(bits)), lower, 0.0)
-        total = total - dot3_blocks(total, dot3_blocks(off, total, mask), mask)
-    return total
-
-
-def state_before(g, keys, vals, state, bbeta, bdecay, live, mask_ref):
-    mask = mask_ref[...]
+def state_before(gs, between, keys, vals, state, bbeta, bdecay, live, mask_ref):
     r = iota((64, 256), 0)
     lane = iota((64, 256), 1)
     c = lane & 63
     pair = lane >> 6
-    n0, n1 = live[2 * g] - 1, live[2 * g + 1] - 1
+    strict = c < r
     lane1 = iota((1, 256), 1)
-    live_row = (lane1 & 63) < jnp.where(lane1 < 128, n0, n1)
-    d_row = jnp.where(live_row, bdecay[g], 0.0)
-    b_row = jnp.where(live_row, bbeta[g], 0.0)
     r1 = iota((256, 128), 0)
-    live_col = (r1 & 63) < jnp.where(r1 < 128, n0, n1)
-    k_all = jnp.where(live_col, keys[pl.ds(2 * g, 2)].astype(F32).reshape(256, 128), 0.0)
-    v_all = jnp.where(live_col, vals[pl.ds(2 * g, 2)].astype(F32).reshape(256, 128), 0.0)
-    kb = k_all.astype(BF16)
-    kt = k_all.T.astype(BF16)
-    b_diag = jnp.where(r == c, b_row, 0.0)
-    d_tri = jnp.where(c <= r, d_row, 0.0)
-    b_col, t_col = [], []
-    for p in range(4):
-        b_col.append(jnp.sum(jnp.where(pair == p, b_diag, 0.0), axis=1, keepdims=True))
-        t_col.append(jnp.sum(jnp.where(pair == p, d_tri, 0.0), axis=1, keepdims=True))
+    zero = jnp.zeros((64, 128), F32)
 
     def side(columns):
         low = jnp.where(pair == 0, columns[0], columns[1])
         high = jnp.where(pair == 2, columns[2], columns[3])
         return jnp.where(pair < 2, low, high)
 
-    tots = side(t_col)
-    tot_row = jnp.sum(jnp.where(r == c, tots, 0.0), axis=0, keepdims=True)
-    strict = c < r
-    fade = jnp.exp(jnp.where(strict, tots - tot_row, 0.0))
-    gram = dot(kb, kt)
-    gram = side([gram[64 * p : 64 * p + 64] for p in range(4)])
-    lower = jnp.where(strict, side(b_col) * gram * fade, 0.0)
-    inverse = unit_inverse(lower, r, c, mask)
-    zero = jnp.zeros((64, 128), F32)
-
     def spread(blocks):
         rows = [[blocks[p] if q == p else zero for q in range(4)] for p in range(4)]
         return jnp.concatenate([jnp.concatenate(row, axis=1) for row in rows], axis=0)
 
-    right = []
-    for p in range(4):
-        at = slice(64 * p, 64 * p + 64)
-        seen = dot2(kb[at], state[2 * g + p // 2, p % 2])
-        right.append(b_col[p] * (v_all[at] - jnp.exp(t_col[p]) * seen))
-    update = dot3(inverse, spread(right))
-    faded = []
-    for p in range(4):
-        faded.append(update[:, 128 * p : 128 * p + 128] * jnp.exp(t_col[p][63:64] - t_col[p]))
-    added = dot2(kt, spread(faded))
-    for p in range(4):
-        end = jnp.exp(t_col[p][63:64])
-        at = (2 * g + p // 2, p % 2)
-        state[at] = end * state[at] + added[:, 128 * p : 128 * p + 128]
+    def prepare(g):
+        n0, n1 = live[2 * g] - 1, live[2 * g + 1] - 1
+        live_row = (lane1 & 63) < jnp.where(lane1 < 128, n0, n1)
+        d_row = jnp.where(live_row, bdecay[g], 0.0)
+        b_row = jnp.where(live_row, bbeta[g], 0.0)
+        live_col = (r1 & 63) < jnp.where(r1 < 128, n0, n1)
+        k_all = jnp.where(live_col, keys[2 * g : 2 * g + 2].astype(F32).reshape(256, 128), 0.0)
+        kb = k_all.astype(BF16)
+        kt = k_all.T.astype(BF16)
+        b_diag = jnp.where(r == c, b_row, 0.0)
+        d_tri = jnp.where(c <= r, d_row, 0.0)
+        b_col, t_col = [], []
+        for p in range(4):
+            b_col.append(jnp.sum(jnp.where(pair == p, b_diag, 0.0), axis=1, keepdims=True))
+            t_col.append(jnp.sum(jnp.where(pair == p, d_tri, 0.0), axis=1, keepdims=True))
+        tots = side(t_col)
+        tot_row = jnp.sum(jnp.where(r == c, tots, 0.0), axis=0, keepdims=True)
+        fade = jnp.exp(jnp.where(strict, tots - tot_row, 0.0))
+        gram = dot(kb, kt)
+        gram = side([gram[64 * p : 64 * p + 64] for p in range(4)])
+        lower = jnp.where(strict, side(b_col) * gram * fade, 0.0)
+        return kb, kt, live_col, b_col, t_col, lower
+
+    def same(bits):
+        return (r >> bits) == (c >> bits)
+
+    prepared = [prepare(g) for g in gs]
+    lowers = [one[5] for one in prepared]
+    mask = mask_ref[...]
+    ident = jnp.where(r == c, 1.0, 0.0)
+    powers = [jnp.where(same(3), -lower, 0.0) for lower in lowers]
+    totals = [ident + power for power in powers]
+    for _ in range(2):
+        powers = [dot3_blocks(power, power, mask) for power in powers]
+        more = [dot3_blocks(total, power, mask) for total, power in zip(totals, powers)]
+        totals = [total + one for total, one in zip(totals, more)]
+    between()
+    for bits in (3, 4, 5):
+        off = same(bits + 1) & jnp.logical_not(same(bits))
+        offs = [jnp.where(off, lower, 0.0) for lower in lowers]
+        offs = [dot3_blocks(one, total, mask) for one, total in zip(offs, totals)]
+        more = [dot3_blocks(total, one, mask) for one, total in zip(offs, totals)]
+        totals = [total - one for total, one in zip(totals, more)]
+    rights = []
+    for g, (kb, _, live_col, b_col, t_col, _) in zip(gs, prepared):
+        v_all = jnp.where(live_col, vals[2 * g : 2 * g + 2].astype(F32).reshape(256, 128), 0.0)
+        right = []
+        for p in range(4):
+            at = slice(64 * p, 64 * p + 64)
+            seen = dot2(kb[at], state[2 * g + p // 2, p % 2])
+            right.append(b_col[p] * (v_all[at] - jnp.exp(t_col[p]) * seen))
+        rights.append(spread(right))
+    updates = [dot3(total, right) for total, right in zip(totals, rights)]
+    added = []
+    for update, (_, kt, _, _, t_col, _) in zip(updates, prepared):
+        faded = []
+        for p in range(4):
+            faded.append(update[:, 128 * p : 128 * p + 128] * jnp.exp(t_col[p][63:64] - t_col[p]))
+        added.append(dot2(kt, spread(faded)))
+    for g, one, (_, _, _, _, t_col, _) in zip(gs, added, prepared):
+        for p in range(4):
+            end = jnp.exp(t_col[p][63:64])
+            at = (2 * g + p // 2, p % 2)
+            state[at] = end * state[at] + one[:, 128 * p : 128 * p + 128]
 
 
 def kernel(
@@ -231,6 +241,30 @@
             device_id_type=pl.DeviceIdType.MESH,
         )
 
+    up_z = ((z + 1) % nz) * NX + x
+    down_z = ((z + nz - 1) % nz) * NX + x
+    barrier = pltpu.get_barrier_semaphore()
+
+    def greet(sem, kv_to, tp_to):
+        pl.semaphore_signal(
+            sem,
+            inc=1,
+            device_id={"kv": kv_to, "tp": tp_to},
+            device_id_type=pl.DeviceIdType.MESH,
+        )
+
+    near_z = [((z + d) % nz) * NX + x for d in (1, nz - 1, 2, nz - 2)]
+    for to in near_z:
+        greet(barrier, to, tp)
+    for d in range(1, NX):
+        greet(barrier, z * NX + (x + d) % NX, tp)
+
+    def greet_tp(d, carry):
+        greet(barrier, kv, (tp + d) % n_tp)
+        return carry
+
+    lax.fori_loop(1, n_tp, greet_tp, 0)
+
     in_tok = local(tok_hbm, tokx.at[x], 12)
     in_gain = local(ngain_hbm, gp.at[x], 13)
     in_w = [local(w, wst.at[i], i) for i, w in enumerate((qw_hbm, kw_hbm, vw_hbm, gw_hbm))]
@@ -256,30 +290,6 @@
         local(mgain_hbm, mgain_ref, 19),
     ]
 
-    up_z = ((z + 1) % nz) * NX + x
-    down_z = ((z + nz - 1) % nz) * NX + x
-    barrier = pltpu.get_barrier_semaphore()
-
-    def greet(sem, kv_to, tp_to):
-        pl.semaphore_signal(
-            sem,
-            inc=1,
-            device_id={"kv": kv_to, "tp": tp_to},
-            device_id_type=pl.DeviceIdType.MESH,
-        )
-
-    near_z = [((z + d) % nz) * NX + x for d in (1, nz - 1, 2, nz - 2)]
-    for to in near_z:
-        greet(barrier, to, tp)
-    for d in range(1, NX):
-        greet(barrier, z * NX + (x + d) % NX, tp)
-
-    def greet_tp(d, carry):
-        greet(barrier, kv, (tp + d) % n_tp)
-        return carry
-
-    lax.fori_loop(1, n_tp, greet_tp, 0)
-
     def round_send(i):
         for to in near_z:
             greet(round_r.at[i], to, tp)
@@ -287,21 +297,11 @@
     def round_wait(i):
         pl.semaphore_wait(round_r.at[i], 4)
 
-    mask[...] = jnp.where((iota((256, 256), 0) >> 6) == (iota((256, 256), 1) >> 6), 1.0, 0.0).astype(
-        BF16
-    )
     in_tok.wait()
     in_gain.wait()
-    tokl[...] = tokx[x].astype(F32).T.astype(BF16)
-    tokt[z] = tokl[pl.ds(pl.multiple_of(z * 32, 32), 32), :]
     for copy in in_w:
         copy.wait()
     mine = pl.ds(pl.multiple_of(x * 64, 64), 64)
-    wcat[mine, :] = wst[x]
-    in_out.wait()
-    in_up.wait()
-    in_down.wait()
-
     pl.semaphore_wait(barrier, 4 + NX - 1 + n_tp - 1)
 
     sent_x = []
@@ -319,16 +319,9 @@
     sent_t = []
     for d in range(1, nz):
         to = (z + d) % nz
-        sent_t.append(
-            remote(
-                tokl.at[pl.ds(pl.multiple_of(to * 32, 32), 32), :],
-                tokt.at[z],
-                ts.at[d],
-                tr.at[d],
-                to * NX + x,
-                tp,
-            )
-        )
+        part = tokl.at[pl.ds(pl.multiple_of(to * 32, 32), 32), :]
+        sent_t.append(remote(part, tokt, ts.at[d], tr, to * NX + x, tp))
+
     def ring(way, step, what):
         to = up_z if way == 0 else down_z
         block = (z + nz - (step - 1)) % nz if way == 0 else (z + step - 1) % nz
@@ -356,6 +349,9 @@
     OUT, UP, LOW, HIGH = 0, 1, 2, 3
 
     round_send(0)
+    in_out.wait()
+    in_up.wait()
+    in_down.wait()
     ring_start(1, OUT)
     ring_start(1, UP)
     ring_start(1, LOW)
@@ -367,15 +363,26 @@
         bbeta[i] = jnp.concatenate([bbeta_ref[pair] for pair in pairs], axis=1)
         bdecay[i] = jnp.concatenate([bdecay_ref[pair] for pair in pairs], axis=1)
 
-    def before(g, carry):
-        state_before(g, keys, vals, state, bbeta, bdecay, live_ref, mask)
-        return carry
-
-    lax.fori_loop(0, 1, before, 0)
-    round_wait(0)
-    round_send(1)
-    ring_pass(1, OUT)
-    lax.fori_loop(1, 2, before, 0)
+    mask[...] = jnp.where((iota((256, 256), 0) >> 6) == (iota((256, 256), 1) >> 6), 1.0, 0.0).astype(
+        BF16
+    )
+    wcat[mine, :] = wst[x]
+    tokl[...] = tokx[x].astype(F32).T.astype(BF16)
+
+    @pl.when(z == tp)
+    def _():
+        tokt[...] = tokl[pl.ds(pl.multiple_of(z * 32, 32), 32), :]
+
+
+    def before(gs, between):
+        state_before(gs, between, keys, vals, state, bbeta, bdecay, live_ref, mask)
+
+    def early():
+        round_wait(0)
+        round_send(1)
+        ring_pass(1, OUT)
+
+    before((0, 1), early)
 
     for copy in sent_x:
         copy.wait_recv()
@@ -397,12 +404,13 @@
     proj_r[kv] = proj_s[kv]
     ex_r[z] = ex_s[kv]
 
-    def send_proj(d, carry):
-        far = d // NX
-        far = nz // 2 + (far + 1) // 2 * (1 - 2 * (far % 2))
-        to = ((z + far) % nz) * NX + (x + NX - 1 - d % NX) % NX
-        remote(proj_s.at[to], proj_r.at[kv], ps.at[0], pr.at[0], to, tp).start()
-        return carry
+    sent_p = []
+    for far in (4, 3, 5, 2, 6, 1, 7, 0):
+        row = ((z + far) % nz) * NX
+        for side in range(NX):
+            if far or side:
+                to = row + (x + side) % NX
+                sent_p.append(remote(proj_s.at[to], proj_r.at[kv], ps.at[0], pr.at[0], to, tp))
 
     def send_extra(d, carry):
         to = ((z + d) % nz) * NX + x
@@ -411,17 +419,20 @@
 
     round_wait(1)
     lax.fori_loop(1, nz, send_extra, 0)
-    lax.fori_loop(0, n_kv - 1, send_proj, 0)
+    for copy in sent_p:
+        copy.start()
+    ring_pass(2, OUT)
     ring_pass(1, UP)
-    lax.fori_loop(2, 3, before, 0)
-    ring_pass(2, OUT)
+    ring_start(1, HIGH)
+    before((2, 3), lambda: None)
+
+    @pl.when(z == tp)
+    def _():
+        for copy in sent_t:
+            copy.start()
+
+    ring_pass(3, OUT)
     ring_pass(1, LOW)
-    ring_start(1, HIGH)
-    lax.fori_loop(3, 4, before, 0)
-    ring_pass(3, OUT)
-    ring_pass(2, UP)
-    for copy in sent_t:
-        copy.start()
 
     some = pl.ds(0, n_kv - 1)
     few = pl.ds(0, nz - 1)
@@ -483,7 +494,7 @@
         sent_m.append(remote(mh.at[x], mh.at[x], ms.at[d], mr.at[d], peer, tp))
     for copy in sent_m:
         copy.start()
-    ring_pass(2, LOW)
+    ring_pass(2, UP)
     for h in range(2):
         e = heads[h][4]
         for s in range(8):
@@ -496,7 +507,15 @@
         copy.wait_recv()
     ring_pass(4, OUT)
     m = mh[...].reshape(32, 256)
-    ar[tp] = dot_nt(m.astype(BF16), out_all[...].reshape(nz * 64, 256)).astype(BF16)
+    partial = dot_nt(m.astype(BF16), out_all[...].reshape(nz * 64, 256))
+
+    @pl.when(z != tp)
+    def _():
+        sent_t[0].wait_recv()
+
+    tokens = jnp.concatenate([tokt[...].astype(F32)] * nz, axis=1)
+    partial = partial + jnp.where((iota((32, 64 * nz), 1) >> 6) == tp, tokens, 0.0)
+    ar[tp] = partial.astype(BF16)
 
     def send_ar(d, carry):
         to = (tp + d) % n_tp
@@ -507,20 +526,17 @@
     ring_pass(3, UP)
     tps = pl.ds(0, n_tp - 1)
     all_ar = remote(ar.at[tps], ar.at[tps], asem, arr, kv, tp)
-    for copy in sent_t:
-        copy.wait_recv()
-    tokens = jnp.concatenate([tokt[i].astype(F32) for i in range(nz)], axis=1)
     gains = []
     for p in range(nz):
         gain = mgain_ref[pl.ds(2 * p + x // 2, 1), :]
         gains.append(jnp.where(x % 2 == 0, gain[:, :64], gain[:, 64:]))
     gains = jnp.concatenate(gains, axis=1)
-    ring_pass(3, LOW)
+    ring_pass(2, LOW)
     all_ar.wait_recv()
     ring_pass(2, HIGH)
 
     attended = jnp.sum(ar[...].astype(F32), axis=0)
-    residual = (tokens + attended).astype(BF16).astype(F32)
+    residual = attended.astype(BF16).astype(F32)
     resid[...] = residual
     squares = jnp.sum(residual * residual, axis=1, keepdims=True)
     mlp_in = (residual * gains).astype(BF16)
@@ -536,6 +552,7 @@
         sent_u.append(remote(ax.at[x], ax.at[x], us.at[d], ur.at[d], peer, tp))
     for copy in sent_u:
         copy.start()
+    ring_pass(3, LOW)
     ring_pass(3, HIGH)
     for copy in sent_u:
         copy.wait_recv()
@@ -555,21 +572,14 @@
 
     lax.fori_loop(1, n_tp, send_rs, 0)
     all_rs = remote(rs.at[tps], rs.at[tps], ds_, dr, kv, tp)
-    all_rs.wait_recv()
-    final = resid[...] + jnp.sum(rs[...].astype(F32), axis=0)
-    for i in range(nz):
-        fin_s[i] = final[:, 64 * i : 64 * i + 64].astype(BF16)
-    mx[z] = fin_s[z]
-
-    sent_f = []
-    for d in range(1, nz):
-        to = (z + d) % nz
-        sent_f.append(remote(fin_s.at[to], mx.at[z], fs.at[d], fr.at[d], to * NX + x, tp))
-    for copy in sent_f:
-        copy.start()
-
-    for copy in sent_x + sent_t + sent_m + sent_u + sent_f:
+    for copy in sent_x + sent_m + sent_u:
         copy.wait_send()
+
+    @pl.when(z == tp)
+    def _():
+        for copy in sent_t:
+            copy.wait_send()
+
     for step in range(1, half + 1):
         for way in range(2):
             for what in (OUT, UP, LOW, HIGH):
@@ -577,18 +587,30 @@
     all_proj.wait_send()
     all_extra.wait_send()
     all_ar.wait_send()
+
+    all_rs.wait_recv()
+    final = resid[...] + jnp.sum(rs[...].astype(F32), axis=0)
+    for i in range(nz):
+        fin_s[i] = final[:, 64 * i : 64 * i + 64].astype(BF16)
+    mx[z] = fin_s[z]
+
+    sent_f = []
+    for d in range(1, nz):
+        to = (z + d) % nz
+        sent_f.append(remote(fin_s.at[to], mx.at[z], fs.at[d], fr.at[d], to * NX + x, tp))
+    for copy in sent_f:
+        copy.start()
+
     all_rs.wait_send()
-
     for copy in sent_f:
-        copy.wait_recv()
+        copy.wait()
     mixed_ref[...] = mx[...].astype(F32).reshape(nz * 32, 64).T.astype(BF16)
 
 
 def put(mixed, state, mixed_hbm, state_hbm, sem):
-    copies = [
-        pltpu.make_async_copy(state, state_hbm, sem.at[0]),
-        pltpu.make_async_copy(mixed, mixed_hbm, sem.at[1]),
-    ]
+    copies = [pltpu.make_async_copy(mixed, mixed_hbm, sem.at[8])]
+    for i in range(8):
+        copies.append(pltpu.make_async_copy(state.at[i], state_hbm.at[i], sem.at[i]))
     for copy in copies:
         copy.start()
     for copy in copies:
@@ -660,7 +682,7 @@
             pltpu.VMEM((NX, 64, 256), BF16),
             pltpu.VMEM((NX, 1, 64), F32),
             pltpu.VMEM((256, 64), BF16),
-            pltpu.VMEM((nz, 32, 64), BF16),
+            pltpu.VMEM((32, 64), BF16),
             pltpu.SMEM((2,), F32),
             pltpu.VMEM((1, 128), F32),
             pltpu.VMEM((8, 2, 64), F32),
@@ -690,7 +712,7 @@
             dma((3, NX)),
             dma((3, NX)),
             dma((nz,)),
-            dma((nz,)),
+            dma,
             dma((2,)),
             dma((2,)),
             dma((NX,)),
@@ -720,7 +742,7 @@
         ),
         in_specs=[vmem, vmem],
         out_specs=(hbm, hbm),
-        scratch_shapes=[dma((2,))],
+        scratch_shapes=[dma((9,))],
         compiler_params=pltpu.CompilerParams(vmem_limit_bytes=16 * 1024 * 1024),
         name="put",
     )(mixed, new_state)

time: 54.4 us -> 53.6 us (0.985)
  Pallas kernels: 53.7 us -> 52.8 us
    pallas_call x1, Pallas kernels: 52.7 us -> 51.8 us  [body(): pl.pallas_call(functools.partial(kernel, n_kv=n_kv, n_tp=n_tp), out_shape...]
where the time goes in v5:
time: 53.6 us; the launch traced here: 53.5 us
  Pallas kernels  52.8 us (99%)
  between operations  0.65 us (1%)
    pallas_call x1, Pallas kernels, body(): pl.pallas_call(functools.partial(kernel, n_kv=n_kv, n_tp=n_tp), out_shape...  51.8 us

profile of v5, /device:TPU:1, one launch (start us, length us, event | category | flops | bytes accessed | tf_op | source)
XLA Modules:
  0.0 53.5 jit_solution(15386704079290726338)
XLA Ops:
  0.6 51.8 %layer.1 = (bf16[64,256]{1,0:T(8,128)(2,1)S(1)}, f32[8,2,128,128]{3,2,1,0:T(8,128)S(1)}) custom-call(bf16[64,256]{1,0:T(8,128)(2,1)} %bitcast.12, f32[1,64]{1,0:T(1,128)} %bitcast.15, bf16[64,256]{1,0:T(8,128)(2,1)} %qw_hbm.1, bf16[64,256]{1,0:T(8,128)(2,1)} %kw_hbm.1, bf16[64,256]{1,0:T(8,128)(2,1)} %vw_hbm.1, bf16[64,256]{1,0:T(8,128)(2,1)} %gw_hbm.1, ...), custom_call_target="tpu_custom_call" | custom-call | tf_op jit(solution)/shard_map/layer/pallas_call | solution.py:670
  52.4 1.0 %put.1 = (bf16[64,256]{1,0:T(8,128)(2,1)}, f32[8,2,128,128]{3,2,1,0:T(8,128)}) custom-call(bf16[64,256]{1,0:T(8,128)(2,1)S(1)} %get-tuple-element.6.mixed, f32[8,2,128,128]{3,2,1,0:T(8,128)S(1)} %get-tuple-element.7.state), custom_call_target="tpu_custom_call" | custom-call | tf_op jit(solution)/shard_map/put/pallas_call | solution.py:737

commit v6 on v5

--- a/solution.py
+++ b/solution.py
@@ -265,29 +265,29 @@
 
     lax.fori_loop(1, n_tp, greet_tp, 0)
 
-    in_tok = local(tok_hbm, tokx.at[x], 12)
-    in_gain = local(ngain_hbm, gp.at[x], 13)
-    in_w = [local(w, wst.at[i], i) for i, w in enumerate((qw_hbm, kw_hbm, vw_hbm, gw_hbm))]
-    in_out = local(out_hbm, out_all.at[z], 6)
-    in_up = local(up_hbm, up_all.at[z], 7)
-    in_down = local(down_hbm, down_all.at[z], 8)
+    in_tok = local(tok_hbm, tokx.at[x], 2)
+    in_gain = local(ngain_hbm, gp.at[x], 3)
+    in_w = [local(w, wst.at[i], 0) for i, w in enumerate((qw_hbm, kw_hbm, vw_hbm, gw_hbm))]
+    in_out = local(out_hbm, out_all.at[z], 4)
+    in_up = local(up_hbm, up_all.at[z], 5)
+    in_down = local(down_hbm, down_all.at[z], 6)
     lanes_z = pl.ds(pl.multiple_of(z * 256, 256), 256)
     in_b = [
-        local(bw_hbm.at[:, lanes_z], bdw.at[0], 4),
-        local(dw_hbm.at[:, lanes_z], bdw.at[1], 5),
+        local(bw_hbm.at[:, lanes_z], bdw.at[0], 1),
+        local(dw_hbm.at[:, lanes_z], bdw.at[1], 1),
     ]
     in_block = [
-        local(bbeta_hbm, bbeta_ref, 14),
-        local(bdecay_hbm, bdecay_ref, 15),
-        local(live_hbm, live_ref, 16),
-        local(keys_hbm, keys, 9),
-        local(vals_hbm, vals, 10),
-        local(state_hbm, state, 11),
+        local(bbeta_hbm, bbeta_ref, 7),
+        local(bdecay_hbm, bdecay_ref, 8),
+        local(live_hbm, live_ref, 9),
+        local(keys_hbm, keys, 10),
+        local(vals_hbm, vals, 11),
+        local(state_hbm, state, 12),
     ]
     in_small = [
-        local(rate_hbm, rate_ref, 17),
-        local(hgain_hbm, hgain_ref, 18),
-        local(mgain_hbm, mgain_ref, 19),
+        local(rate_hbm, rate_ref, 13),
+        local(hgain_hbm, hgain_ref, 14),
+        local(mgain_hbm, mgain_ref, 15),
     ]
 
     def round_send(i):
@@ -299,8 +299,7 @@
 
     in_tok.wait()
     in_gain.wait()
-    for copy in in_w:
-        copy.wait()
+    pltpu.make_async_copy(wst, wst, loc.at[0]).wait()
     mine = pl.ds(pl.multiple_of(x * 64, 64), 64)
     pl.semaphore_wait(barrier, 4 + NX - 1 + n_tp - 1)
 
@@ -308,11 +307,9 @@
     for d in range(1, NX):
         to = (x + d) % NX
         peer = z * NX + to
-        sent_x.append(remote(tokx.at[x], tokx.at[x], xs.at[0, d], xr.at[0, d], peer, tp))
-        sent_x.append(remote(gp.at[x], gp.at[x], xs.at[1, d], xr.at[1, d], peer, tp))
-        sent_x.append(
-            remote(wst.at[to], wcat.at[mine, :], xs.at[2, d], xr.at[2, d], peer, tp)
-        )
+        sent_x.append(remote(tokx.at[x], tokx.at[x], xs.at[0], xr.at[0], peer, tp))
+        sent_x.append(remote(gp.at[x], gp.at[x], xs.at[1], xr.at[1], peer, tp))
+        sent_x.append(remote(wst.at[to], wcat.at[mine, :], xs.at[2], xr.at[2], peer, tp))
     for copy in sent_x:
         copy.start()
 
@@ -320,7 +317,7 @@
     for d in range(1, nz):
         to = (z + d) % nz
         part = tokl.at[pl.ds(pl.multiple_of(to * 32, 32), 32), :]
-        sent_t.append(remote(part, tokt, ts.at[d], tr, to * NX + x, tp))
+        sent_t.append(remote(part, tokt, ts, tr, to * NX + x, tp))
 
     def ring(way, step, what):
         to = up_z if way == 0 else down_z
@@ -331,7 +328,7 @@
             first, rows = first + rows // 2 * way, rows // 2
         ref = ref.at[pl.ds(first, rows)]
         return remote(
-            ref, ref, ring_s.at[way, step - 1, what], ring_r.at[way, step - 1, what], to, tp
+            ref, ref, ring_s.at[min(what, 2)], ring_r.at[way, step - 1, what], to, tp
         )
 
     half = nz // 2
@@ -384,14 +381,23 @@
 
     before((0, 1), early)
 
-    for copy in sent_x:
+    three = pl.ds(0, NX - 1)
+
+    def whole(ref, s, r):
+        return remote(ref, ref, s, r, kv, tp)
+
+    all_x = [
+        whole(tokx.at[three], xs.at[0], xr.at[0]),
+        whole(gp.at[three], xs.at[1], xr.at[1]),
+        whole(wst.at[three], xs.at[2], xr.at[2]),
+    ]
+    for copy in all_x:
         copy.wait_recv()
     t = tokx[...].reshape(256, 256).astype(F32).T
     squares = jnp.sum(t * t, axis=1, keepdims=True)
     normed = (t * jnp.concatenate([gp[i] for i in range(NX)], axis=1)).astype(BF16)
     projected = dot(normed, wcat[...])
-    for copy in in_b:
-        copy.wait()
+    pltpu.make_async_copy(bdw, bdw, loc.at[1]).wait()
     small = jnp.concatenate(
         [bdw[...].astype(F32).reshape(32, 256), jnp.zeros((96, 256), F32)], axis=0
     ).astype(BF16)
@@ -491,7 +497,7 @@
     sent_m = []
     for d in range(1, NX):
         peer = z * NX + (x + d) % NX
-        sent_m.append(remote(mh.at[x], mh.at[x], ms.at[d], mr.at[d], peer, tp))
+        sent_m.append(remote(mh.at[x], mh.at[x], ms, mr, peer, tp))
     for copy in sent_m:
         copy.start()
     ring_pass(2, UP)
@@ -503,8 +509,8 @@
 
     ring_pass(1, HIGH)
 
-    for copy in sent_m:
-        copy.wait_recv()
+    all_m = whole(mh.at[three], ms, mr)
+    all_m.wait_recv()
     ring_pass(4, OUT)
     m = mh[...].reshape(32, 256)
     partial = dot_nt(m.astype(BF16), out_all[...].reshape(nz * 64, 256))
@@ -537,7 +543,8 @@
 
     attended = jnp.sum(ar[...].astype(F32), axis=0)
     residual = attended.astype(BF16).astype(F32)
-    resid[...] = residual
+    for i in range(nz):
+        resid[i] = residual[:, 64 * i : 64 * i + 64]
     squares = jnp.sum(residual * residual, axis=1, keepdims=True)
     mlp_in = (residual * gains).astype(BF16)
     ring_pass(4, UP)
@@ -549,61 +556,71 @@
     sent_u = []
     for d in range(1, NX):
         peer = z * NX + (x + d) % NX
-        sent_u.append(remote(ax.at[x], ax.at[x], us.at[d], ur.at[d], peer, tp))
+        sent_u.append(remote(ax.at[x], ax.at[x], us, ur, peer, tp))
     for copy in sent_u:
         copy.start()
     ring_pass(3, LOW)
     ring_pass(3, HIGH)
-    for copy in sent_u:
-        copy.wait_recv()
-    ring_pass(4, LOW)
-    ring_pass(4, HIGH)
+    all_u = whole(ax.at[three], us, ur)
+    all_u.wait_recv()
     total = jnp.sum(ax[...].astype(F32), axis=0)
     rms = lax.rsqrt((total[:, 1024:1025] + total[:, 1025:1026]) / MODEL + EPS)
     hidden = jnp.maximum(total[:, :1024] * rms, 0.0)
     hidden = (hidden * hidden).astype(BF16)
-    output = dot_nt(hidden, down_all[...].reshape(nz * 64, 1024))
-    rs[tp] = output.astype(BF16)
-
-    def send_rs(d, carry):
-        to = (tp + d) % n_tp
-        remote(rs.at[tp], rs.at[tp], ds_, dr, kv, to).start()
-        return carry
-
-    lax.fori_loop(1, n_tp, send_rs, 0)
-    all_rs = remote(rs.at[tps], rs.at[tps], ds_, dr, kv, tp)
-    for copy in sent_x + sent_m + sent_u:
+    near, distant = (0, 1, 7, 2), (6, 3, 5, 4)
+
+    def project(half, places):
+        for i in range(0, 4, 2):
+            pair = [down_all[(z + places[j]) % nz] for j in (i, i + 1)]
+            part = dot_nt(hidden, jnp.concatenate(pair, axis=0))
+            rs[half, tp, :, 64 * i : 64 * i + 128] = part.astype(BF16)
+
+        def send_rs(d, carry):
+            to = (tp + d) % n_tp
+            remote(rs.at[half, tp], rs.at[half, tp], ds_.at[half], dr.at[half], kv, to).start()
+            return carry
+
+        lax.fori_loop(1, n_tp, send_rs, 0)
+
+    project(0, near)
+    ring_pass(4, LOW)
+    ring_pass(4, HIGH)
+    project(1, distant)
+    all_rs = [
+        remote(rs.at[i, tps], rs.at[i, tps], ds_.at[i], dr.at[i], kv, tp) for i in range(2)
+    ]
+
+    for copy in all_x + [all_m, all_u]:
         copy.wait_send()
 
     @pl.when(z == tp)
     def _():
-        for copy in sent_t:
-            copy.wait_send()
-
-    for step in range(1, half + 1):
-        for way in range(2):
-            for what in (OUT, UP, LOW, HIGH):
-                ring(way, step, what).wait_send()
+        whole(tokl.at[pl.ds(0, 32 * (nz - 1)), :], ts, tr).wait_send()
+
+    for ref, sem in zip((out_all, up_all, down_all), range(3)):
+        whole(ref.at[few], ring_s.at[sem], tr).wait_send()
     all_proj.wait_send()
     all_extra.wait_send()
     all_ar.wait_send()
 
-    all_rs.wait_recv()
-    final = resid[...] + jnp.sum(rs[...].astype(F32), axis=0)
-    for i in range(nz):
-        fin_s[i] = final[:, 64 * i : 64 * i + 64].astype(BF16)
-    mx[z] = fin_s[z]
-
     sent_f = []
-    for d in range(1, nz):
-        to = (z + d) % nz
-        sent_f.append(remote(fin_s.at[to], mx.at[z], fs.at[d], fr.at[d], to * NX + x, tp))
-    for copy in sent_f:
-        copy.start()
-
-    all_rs.wait_send()
-    for copy in sent_f:
-        copy.wait()
+    for half, places in enumerate((near, distant)):
+        all_rs[half].wait_recv()
+        added = jnp.sum(rs[half].astype(F32), axis=0)
+        for i, place in enumerate(places):
+            to = (z + place) % nz
+            row = resid[to] + added[:, 64 * i : 64 * i + 64]
+            fin_s[to] = row.astype(BF16)
+            if place:
+                copy = remote(fin_s.at[to], mx.at[z], fs, fr, to * NX + x, tp)
+                copy.start()
+                sent_f.append(copy)
+            else:
+                mx[z] = fin_s[z]
+    all_f = whole(fin_s.at[few], fs, fr)
+    for copy in all_rs:
+        copy.wait_send()
+    all_f.wait()
     mixed_ref[...] = mx[...].astype(F32).reshape(nz * 32, 64).T.astype(BF16)
 
 
@@ -704,28 +721,28 @@
             pltpu.VMEM((NX, 8, 256), F32),
             pltpu.VMEM((n_tp, 32, 512), BF16),
             pltpu.VMEM((NX, 32, 1152), BF16),
-            pltpu.VMEM((n_tp, 32, 512), BF16),
-            pltpu.VMEM((32, 512), F32),
+            pltpu.VMEM((2, n_tp, 32, 256), BF16),
+            pltpu.VMEM((nz, 32, 64), F32),
             pltpu.VMEM((nz, 32, 64), BF16),
             pltpu.VMEM((nz, 32, 64), BF16),
-            dma((20,)),
-            dma((3, NX)),
-            dma((3, NX)),
-            dma((nz,)),
+            dma((16,)),
+            dma((3,)),
+            dma((3,)),
+            dma,
             dma,
             dma((2,)),
             dma((2,)),
-            dma((NX,)),
-            dma((NX,)),
-            dma,
-            dma,
-            dma((NX,)),
-            dma((NX,)),
-            dma,
-            dma,
-            dma((nz,)),
-            dma((nz,)),
-            dma((2, 4, 4)),
+            dma,
+            dma,
+            dma,
+            dma,
+            dma,
+            dma,
+            dma((2,)),
+            dma((2,)),
+            dma,
+            dma,
+            dma((3,)),
             dma((2, 4, 4)),
             pltpu.SemaphoreType.REGULAR((2,)),
         ],

time: 53.6 us -> 52.8 us (0.985)
  Pallas kernels: 52.8 us -> 52 us
    pallas_call x1, Pallas kernels: 51.8 us -> 51 us  [body(): pl.pallas_call(functools.partial(kernel, n_kv=n_kv, n_tp=n_tp), out_shape...]
where the time goes in v6:
time: 52.8 us; the launch traced here: 52.7 us
  Pallas kernels  52 us (98%)
  between operations  0.65 us (1%)
    pallas_call x1, Pallas kernels, body(): pl.pallas_call(functools.partial(kernel, n_kv=n_kv, n_tp=n_tp), out_shape...  51 us

profile of v6, /device:TPU:1, one launch (start us, length us, event | category | flops | bytes accessed | tf_op | source)
XLA Modules:
  0.0 52.7 jit_solution(10801308381317846543)
XLA Ops:
  0.6 51.0 %layer.1 = (bf16[64,256]{1,0:T(8,128)(2,1)S(1)}, f32[8,2,128,128]{3,2,1,0:T(8,128)S(1)}) custom-call(bf16[64,256]{1,0:T(8,128)(2,1)} %bitcast.12, f32[1,64]{1,0:T(1,128)} %bitcast.15, bf16[64,256]{1,0:T(8,128)(2,1)} %qw_hbm.1, bf16[64,256]{1,0:T(8,128)(2,1)} %kw_hbm.1, bf16[64,256]{1,0:T(8,128)(2,1)} %vw_hbm.1, bf16[64,256]{1,0:T(8,128)(2,1)} %gw_hbm.1, ...), custom_call_target="tpu_custom_call" | custom-call | tf_op jit(solution)/shard_map/layer/pallas_call | solution.py:687
  51.6 1.0 %put.1 = (bf16[64,256]{1,0:T(8,128)(2,1)}, f32[8,2,128,128]{3,2,1,0:T(8,128)}) custom-call(bf16[64,256]{1,0:T(8,128)(2,1)S(1)} %get-tuple-element.6.mixed, f32[8,2,128,128]{3,2,1,0:T(8,128)S(1)} %get-tuple-element.7.state), custom_call_target="tpu_custom_call" | custom-call | tf_op jit(solution)/shard_map/put/pallas_call | solution.py:754

commit v7 on v6

--- a/solution.py
+++ b/solution.py
@@ -377,6 +377,12 @@
     def early():
         round_wait(0)
         round_send(1)
+
+        @pl.when(z == tp)
+        def _():
+            for copy in sent_t:
+                copy.start()
+
         ring_pass(1, OUT)
 
     before((0, 1), early)
@@ -431,11 +437,6 @@
     ring_pass(1, UP)
     ring_start(1, HIGH)
     before((2, 3), lambda: None)
-
-    @pl.when(z == tp)
-    def _():
-        for copy in sent_t:
-            copy.start()
 
     ring_pass(3, OUT)
     ring_pass(1, LOW)

time: 52.8 us -> 51.5 us (0.975)
  Pallas kernels: 52 us -> 50.7 us
    pallas_call x1, Pallas kernels: 51 us -> 49.7 us  [body(): pl.pallas_call(functools.partial(kernel, n_kv=n_kv, n_tp=n_tp), out_shape...]
where the time goes in v7:
time: 51.5 us; the launch traced here: 51.4 us
  Pallas kernels  50.7 us (98%)
  between operations  0.65 us (1%)
    pallas_call x1, Pallas kernels, body(): pl.pallas_call(functools.partial(kernel, n_kv=n_kv, n_tp=n_tp), out_shape...  49.7 us
    pallas_call x1, Pallas kernels, body(): pl.pallas_call(put, out_shape=(jax.ShapeDtypeStruct(mixed.shape, BF16), j...  1.05 us

profile of v7, /device:TPU:1, one launch (start us, length us, event | category | flops | bytes accessed | tf_op | source)
XLA Modules:
  0.0 51.4 jit_solution(5914945986720608651)
XLA Ops:
  0.6 49.7 %layer.1 = (bf16[64,256]{1,0:T(8,128)(2,1)S(1)}, f32[8,2,128,128]{3,2,1,0:T(8,128)S(1)}) custom-call(bf16[64,256]{1,0:T(8,128)(2,1)} %bitcast.12, f32[1,64]{1,0:T(1,128)} %bitcast.15, bf16[64,256]{1,0:T(8,128)(2,1)} %qw_hbm.1, bf16[64,256]{1,0:T(8,128)(2,1)} %kw_hbm.1, bf16[64,256]{1,0:T(8,128)(2,1)} %vw_hbm.1, bf16[64,256]{1,0:T(8,128)(2,1)} %gw_hbm.1, ...), custom_call_target="tpu_custom_call" | custom-call | tf_op jit(solution)/shard_map/layer/pallas_call | solution.py:688
  50.3 1.0 %put.1 = (bf16[64,256]{1,0:T(8,128)(2,1)}, f32[8,2,128,128]{3,2,1,0:T(8,128)}) custom-call(bf16[64,256]{1,0:T(8,128)(2,1)S(1)} %get-tuple-element.6.mixed, f32[8,2,128,128]{3,2,1,0:T(8,128)S(1)} %get-tuple-element.7.state), custom_call_target="tpu_custom_call" | custom-call | tf_op jit(solution)/shard_map/put/pallas_call | solution.py:755

commit v8 on v7

--- a/solution.py
+++ b/solution.py
@@ -192,6 +192,7 @@
     mh,
     ar,
     ax,
+    sq,
     rs,
     resid,
     fin_s,
@@ -209,6 +210,8 @@
     arr,
     us,
     ur,
+    sqs,
+    sqr,
     ds_,
     dr,
     fs,
@@ -322,13 +325,13 @@
     def ring(way, step, what):
         to = up_z if way == 0 else down_z
         block = (z + nz - (step - 1)) % nz if way == 0 else (z + step - 1) % nz
-        ref = (out_all, up_all, down_all, down_all)[what].at[block]
-        first, rows = (0, 64) if what < 2 else (32 * (what - 2), 32)
+        ref = (out_all, up_all, up_all, down_all, down_all)[what].at[block]
+        first, rows = (0, 64) if what == 0 else (32 * ((what - 1) % 2), 32)
         if step == nz // 2:
             first, rows = first + rows // 2 * way, rows // 2
         ref = ref.at[pl.ds(first, rows)]
         return remote(
-            ref, ref, ring_s.at[min(what, 2)], ring_r.at[way, step - 1, what], to, tp
+            ref, ref, ring_s.at[(what + 1) // 2], ring_r.at[way, step - 1, what], to, tp
         )
 
     half = nz // 2
@@ -343,7 +346,7 @@
             if step < half:
                 ring(way, step + 1, what).start()
 
-    OUT, UP, LOW, HIGH = 0, 1, 2, 3
+    OUT, UP, UQ, LOW, HIGH = 0, 1, 2, 3, 4
 
     round_send(0)
     in_out.wait()
@@ -351,6 +354,7 @@
     in_down.wait()
     ring_start(1, OUT)
     ring_start(1, UP)
+    ring_start(1, UQ)
     ring_start(1, LOW)
 
     for copy in in_block:
@@ -433,10 +437,14 @@
     lax.fori_loop(1, nz, send_extra, 0)
     for copy in sent_p:
         copy.start()
-    ring_pass(2, OUT)
-    ring_pass(1, UP)
-    ring_start(1, HIGH)
-    before((2, 3), lambda: None)
+
+    def later():
+        ring_pass(2, OUT)
+        ring_pass(1, UP)
+        ring_pass(1, UQ)
+        ring_start(1, HIGH)
+
+    before((2, 3), later)
 
     ring_pass(3, OUT)
     ring_pass(1, LOW)
@@ -502,6 +510,7 @@
     for copy in sent_m:
         copy.start()
     ring_pass(2, UP)
+    ring_pass(2, UQ)
     for h in range(2):
         e = heads[h][4]
         for s in range(8):
@@ -531,6 +540,7 @@
 
     lax.fori_loop(1, n_tp, send_ar, 0)
     ring_pass(3, UP)
+    ring_pass(3, UQ)
     tps = pl.ds(0, n_tp - 1)
     all_ar = remote(ar.at[tps], ar.at[tps], asem, arr, kv, tp)
     gains = []
@@ -547,13 +557,16 @@
     for i in range(nz):
         resid[i] = residual[:, 64 * i : 64 * i + 64]
     squares = jnp.sum(residual * residual, axis=1, keepdims=True)
+    row = iota((32, 128), 0) == iota((32, 128), 1)
+    sq[x] = jnp.sum(jnp.where(row, squares, 0.0), axis=0, keepdims=True)
+    for d in range(1, NX):
+        remote(sq.at[x], sq.at[x], sqs, sqr, z * NX + (x + d) % NX, tp).start()
+    all_q = whole(sq.at[three], sqs, sqr)
     mlp_in = (residual * gains).astype(BF16)
     ring_pass(4, UP)
+    ring_pass(4, UQ)
     pre = dot(mlp_in, up_all[...].reshape(nz * 64, 1024))
-    high = squares.astype(BF16).astype(F32)
-    lane = iota((32, 128), 1)
-    tail = jnp.where(lane == 0, high, jnp.where(lane == 1, squares - high, 0.0))
-    ax[x] = jnp.concatenate([pre, tail], axis=1).astype(BF16)
+    ax[x] = pre.astype(BF16)
     sent_u = []
     for d in range(1, NX):
         peer = z * NX + (x + d) % NX
@@ -564,9 +577,11 @@
     ring_pass(3, HIGH)
     all_u = whole(ax.at[three], us, ur)
     all_u.wait_recv()
+    all_q.wait_recv()
     total = jnp.sum(ax[...].astype(F32), axis=0)
-    rms = lax.rsqrt((total[:, 1024:1025] + total[:, 1025:1026]) / MODEL + EPS)
-    hidden = jnp.maximum(total[:, :1024] * rms, 0.0)
+    squares = jnp.where(row, jnp.sum(sq[...], axis=0), 0.0)
+    rms = lax.rsqrt(jnp.sum(squares, axis=1, keepdims=True) / MODEL + EPS)
+    hidden = jnp.maximum(total * rms, 0.0)
     hidden = (hidden * hidden).astype(BF16)
     near, distant = (0, 1, 7, 2), (6, 3, 5, 4)
 
@@ -591,7 +606,7 @@
         remote(rs.at[i, tps], rs.at[i, tps], ds_.at[i], dr.at[i], kv, tp) for i in range(2)
     ]
 
-    for copy in all_x + [all_m, all_u]:
+    for copy in all_x + [all_m, all_u, all_q]:
         copy.wait_send()
 
     @pl.when(z == tp)
@@ -721,7 +736,8 @@
             pltpu.VMEM((4, 1, 256), F32),
             pltpu.VMEM((NX, 8, 256), F32),
             pltpu.VMEM((n_tp, 32, 512), BF16),
-            pltpu.VMEM((NX, 32, 1152), BF16),
+            pltpu.VMEM((NX, 32, 1024), BF16),
+            pltpu.VMEM((NX, 1, 128), F32),
             pltpu.VMEM((2, n_tp, 32, 256), BF16),
             pltpu.VMEM((nz, 32, 64), F32),
             pltpu.VMEM((nz, 32, 64), BF16),
@@ -739,12 +755,14 @@
             dma,
             dma,
             dma,
+            dma,
+            dma,
             dma((2,)),
             dma((2,)),
             dma,
             dma,
             dma((3,)),
-            dma((2, 4, 4)),
+            dma((2, 4, 5)),
             pltpu.SemaphoreType.REGULAR((2,)),
         ],
         compiler_params=pltpu.CompilerParams(

time: 51.5 us -> 51.5 us (level)
  no operation moved by 1% of the time
where the time goes in v8:
time: 51.5 us; the launch traced here: 51.4 us
  Pallas kernels  50.8 us (99%)
  between operations  0.65 us (1%)
    pallas_call x1, Pallas kernels, body(): pl.pallas_call(functools.partial(kernel, n_kv=n_kv, n_tp=n_tp), out_shape...  49.7 us
    pallas_call x1, Pallas kernels, body(): pl.pallas_call(put, out_shape=(jax.ShapeDtypeStruct(mixed.shape, BF16), j...  1.05 us

profile of v8, /device:TPU:1, one launch (start us, length us, event | category | flops | bytes accessed | tf_op | source)
XLA Modules:
  0.0 51.4 jit_solution(7677308274740339756)
XLA Ops:
  0.6 49.7 %layer.1 = (bf16[64,256]{1,0:T(8,128)(2,1)S(1)}, f32[8,2,128,128]{3,2,1,0:T(8,128)S(1)}) custom-call(bf16[64,256]{1,0:T(8,128)(2,1)} %bitcast.12, f32[1,64]{1,0:T(1,128)} %bitcast.15, bf16[64,256]{1,0:T(8,128)(2,1)} %qw_hbm.1, bf16[64,256]{1,0:T(8,128)(2,1)} %kw_hbm.1, bf16[64,256]{1,0:T(8,128)(2,1)} %vw_hbm.1, bf16[64,256]{1,0:T(8,128)(2,1)} %gw_hbm.1, ...), custom_call_target="tpu_custom_call" | custom-call | tf_op jit(solution)/shard_map/layer/pallas_call | solution.py:703
  50.4 1.0 %put.1 = (bf16[64,256]{1,0:T(8,128)(2,1)}, f32[8,2,128,128]{3,2,1,0:T(8,128)}) custom-call(bf16[64,256]{1,0:T(8,128)(2,1)S(1)} %get-tuple-element.6.mixed, f32[8,2,128,128]{3,2,1,0:T(8,128)S(1)} %get-tuple-element.7.state), custom_call_target="tpu_custom_call" | custom-call | tf_op jit(solution)/shard_map/put/pallas_call | solution.py:773
